TPU v7x, 512 devices: a 4x2x32 block of a 4x8x32 slice. The times are simulated.
512 devices in a mesh: grp: 2 (over y), tp: 32 (over z), dp: 8 (over x, core).
Axes of the slice: x: 4, y: 2, z: 32, core: 2. Of those that a mesh axis runs over, the one named last changes fastest.
The devices are a block of a 4x8x32 slice.
Arguments:
- residual_token_input: bfloat16 [128, 4096], P('grp', 'dp'), parts along dimension 0, may hold values from -64 to 64
- sequence_token_count: int32 [128], P(('grp', 'dp')), parts along dimension 0, may hold values from 1 to 16, 256 in all
- input_norm_gain: float32 [2, 4096], P(None, 'dp'), may hold values from 0.1 to 1.9
- value_projection: bfloat16 [2, 4096, 4096], P(None, 'dp', 'tp'), may hold values from -0.09375 to 0.09375
- input_key_projection: bfloat16 [2, 4096, 4096], P(None, 'dp', 'tp'), may hold values from -0.09375 to 0.09375
- readout_key_projection: bfloat16 [2, 4096, 4096], P(None, 'dp', 'tp'), may hold values from -0.09375 to 0.09375
- gate_projection: bfloat16 [2, 4096, 4096], P(None, 'dp', 'tp'), may hold values from -0.09375 to 0.09375
- step_size_projection: bfloat16 [2, 4096, 64], P(None, 'dp'), may hold values from -0.09375 to 0.09375
- convolution_weights: bfloat16 [2, 5, 3, 4096], P(None, None, None, 'tp'), may hold values from -2.5 to 2.5
- convolution_history: bfloat16 [2, 128, 4, 3, 4096], P(None, ('grp', 'dp'), None, None, 'tp'), parts along dimension 1, may hold values from -6 to 6
- step_size_bias: float32 [2, 64], P(None, 'tp'), may hold values from -4.6 to -1.5
- head_decay_logarithm: float32 [2, 64], P(None, 'tp'), may hold values from 0 to 2.77
- direct_path_gain: float32 [2, 64], P(None, 'tp'), may hold values from 0.1 to 1.9
- extra_decay_logarithm: float32 [2, 128, 64], P(None, ('grp', 'dp'), 'tp'), parts along dimension 1, may hold values from -0.7 to 0
- recurrent_state: float32 [2, 128, 64, 64, 128], P(None, ('grp', 'dp'), 'tp'), parts along dimension 1, may hold values from -1.5 to 1.5
- output_norm_gain: float32 [2, 4096], P(None, 'tp'), may hold values from 0.1 to 1.9
- output_projection: bfloat16 [2, 4096, 4096], P(None, 'tp', 'dp'), may hold values from -0.09375 to 0.09375
Outputs:
- hidden_out: bfloat16 [128, 4096], P(('grp', 'tp'), 'dp'), parts along dimension 0
- state_out: float32 [2, 128, 64, 64, 128], P(None, ('grp', 'dp'), 'tp'), parts along dimension 1
- window_out: bfloat16 [2, 128, 4, 3, 4096], P(None, ('grp', 'dp'), None, None, 'tp'), parts along dimension 1
There are 2 independent parts, one for each index of `grp`. A program takes and returns all parts, laid end to end along the dimension named above; an argument that names none is the same for every part. Nothing has to cross between parts.
Inputs may be any that keep to these rules, and one draw needn't show every extreme that they name: `sequence_token_count`: tokens already in each sequence before this step.
All inputs are finite; a program needn't handle non-finite values. No bound on the sum of `sequence_token_count` on one device may be relied on, other than what follows from the above.
Results may differ from a plain program's by a relative error of at most 0.015.
Values may be sent and summed in bfloat16 or wider, within the bound.
A program may use at most 64 MiB of HBM per device.

v0:
```python
import math

import jax
import jax.numpy as jnp
from jax import lax
from jax.sharding import PartitionSpec as P

D = 4096
HEADS = 64
HEAD_DIM = 64
GROUPS = 32
LAYERS = 2


EPSILON = 1e-06


def split_up(shard, dim, devices):
    before, after = (shard.shape[:dim], shard.shape[dim + 1 :])
    return jnp.moveaxis(shard.reshape(*before, devices, -1, *after), dim, 0)


def sum_at_owner(shard, axis, dim):
    blocks = split_up(shard, dim, lax.axis_size(axis))
    arrived = lax.all_to_all(blocks, axis, split_axis=0, concat_axis=0, tiled=True)
    return arrived.sum(axis=0)


def in_one_piece(arrays, axis, dim, along):
    widths = [math.prod(a.shape[along:]) for a in arrays]
    both = jnp.concatenate(
        [a.reshape(*a.shape[:along], w) for a, w in zip(arrays, widths)], axis=along
    )
    filled = sum_at_owner(both, axis, dim)
    blocks = jnp.split(filled, [sum(widths[:k]) for k in range(1, len(widths))], axis=along)
    return tuple(
        (b.reshape(*filled.shape[:along], *a.shape[along:]) for a, b in zip(arrays, blocks))
    )


def copy_for_each(shard, axis):
    devices = lax.axis_size(axis)
    return lax.all_to_all(
        jnp.broadcast_to(shard[None], (devices, *shard.shape)), axis, 0, 0, tiled=True
    )


def in_order(blocks, dim):
    blocks = jnp.moveaxis(blocks, 0, dim)
    dims = blocks.shape
    return blocks.reshape(*dims[:dim], dims[dim] * dims[dim + 1], *dims[dim + 2 :])


def gather_directly(shard, axis, dim):
    blocks = copy_for_each(shard, axis)
    return in_order(blocks, dim)


def conv_mixed(current, window_layer, taps_layer, lengths_now):
    taps_float = taps_layer.astype(jnp.float32)
    width_back = window_layer.shape[1]
    steps_back = width_back - jnp.arange(width_back, dtype=jnp.int32)
    live_mask = (steps_back[None, :] <= lengths_now[:, None]).astype(jnp.float32)
    earlier = jnp.sum(
        window_layer.astype(jnp.float32)
        * live_mask[:, :, None, None]
        * taps_float[None, :width_back],
        axis=1,
    )
    return jax.nn.silu(earlier + current.astype(jnp.float32) * taps_float[width_back][None])


def state_after_update(
    layer_recurrent_state,
    layer_extra_decay,
    mixer_input_normed,
    step_size_input,
    layer_bias_slice,
    layer_decay_logarithm,
    layer_direct_gain,
):
    seq_count, heads_here, head_width, state_width = layer_recurrent_state.shape
    groups_here = mixer_input_normed.shape[2] // state_width
    per_group = heads_here // groups_here
    step_size_value = jax.nn.softplus(step_size_input.astype(jnp.float32) + layer_bias_slice[None])
    decay_factor_current = jnp.exp(
        -step_size_value * jnp.exp(layer_decay_logarithm)[None] + layer_extra_decay
    )
    values = mixer_input_normed[:, 0].reshape(seq_count, groups_here, per_group, head_width)
    inkeys = mixer_input_normed[:, 1].reshape(seq_count, groups_here, state_width)
    readkeys = mixer_input_normed[:, 2].reshape(seq_count, groups_here, state_width)
    grouped_state = layer_recurrent_state.reshape(
        seq_count, groups_here, per_group, head_width, state_width
    )
    decay_group = decay_factor_current.reshape(seq_count, groups_here, per_group)
    rate_group = step_size_value.reshape(seq_count, groups_here, per_group)
    skip_group = layer_direct_gain.reshape(groups_here, per_group)
    updated_state = (
        decay_group[..., None, None] * grouped_state
        + (rate_group[..., None] * values)[..., None] * inkeys[:, :, None, None, :]
    )
    readout_key_vector = jnp.einsum("sgrpn,sgn->sgrp", updated_state, readkeys)
    readout_key_vector = readout_key_vector + skip_group[None, :, :, None] * values
    return (
        updated_state.reshape(layer_recurrent_state.shape),
        readout_key_vector.reshape(seq_count, heads_here * head_width),
    )


def group_norm(gated_out, gain_layer, group_width):
    seq_count = gated_out.shape[0]
    grouped = gated_out.reshape(seq_count, -1, group_width)
    scaled = grouped * lax.rsqrt(jnp.mean(grouped * grouped, axis=2, keepdims=True) + EPSILON)
    return (scaled.reshape(seq_count, -1) * gain_layer[None]).astype(jnp.bfloat16)


def project_part(scaled_in, weight):
    return jnp.dot(scaled_in, weight, preferred_element_type=jnp.float32)


def body(
    residual_token_input,
    sequence_token_count,
    input_norm_gain,
    value_projection,
    input_key_projection,
    readout_key_projection,
    gate_projection,
    step_size_projection,
    convolution_weights,
    convolution_history,
    step_size_bias,
    head_decay_logarithm,
    direct_path_gain,
    extra_decay_logarithm,
    recurrent_state,
    output_norm_gain,
    output_projection,
):
    group_width = HEADS * HEAD_DIM // GROUPS
    heads_here = step_size_bias.shape[1]
    head_start = lax.axis_index("tp") * heads_here
    row_count = residual_token_input.shape[0] // lax.axis_size("tp")
    row_start = lax.axis_index("tp") * row_count
    hidden_cols = residual_token_input
    hidden_rows = lax.dynamic_slice_in_dim(residual_token_input, row_start, row_count, 0)
    states_new = []
    windows_new = []
    for layer_position in range(LAYERS):
        hidden_float = hidden_cols.astype(jnp.float32)
        part_squares = jnp.sum(hidden_float * hidden_float, axis=1)
        scaled_in = (hidden_float * input_norm_gain[layer_position][None]).astype(jnp.bfloat16)
        step_weight = lax.dynamic_slice_in_dim(
            step_size_projection[layer_position], head_start, heads_here, 1
        )
        value_sum, inkey_sum, readout_sum, gate_sum, step_sum, square_sum = in_one_piece(
            (
                project_part(scaled_in, value_projection[layer_position]),
                project_part(scaled_in, input_key_projection[layer_position]),
                project_part(scaled_in, readout_key_projection[layer_position]),
                project_part(scaled_in, gate_projection[layer_position]),
                project_part(scaled_in, step_weight),
                part_squares,
            ),
            "dp",
            0,
            1,
        )
        inverse = lax.rsqrt(square_sum / D + EPSILON)[:, None]
        current = jnp.stack(
            [
                (inverse * value_sum).astype(jnp.bfloat16),
                (inverse * inkey_sum).astype(jnp.bfloat16),
                (inverse * readout_sum).astype(jnp.bfloat16),
            ],
            axis=1,
        )
        gate_in = (inverse * gate_sum).astype(jnp.bfloat16)
        step_size_input = (inverse * step_sum).astype(jnp.bfloat16)
        mixer_input_normed = conv_mixed(
            current,
            convolution_history[layer_position],
            convolution_weights[layer_position],
            sequence_token_count,
        )
        windows_new.append(
            jnp.concatenate([convolution_history[layer_position][:, 1:], current[:, None]], axis=1)
        )
        updated_state, readout_key_vector = state_after_update(
            recurrent_state[layer_position],
            extra_decay_logarithm[layer_position],
            mixer_input_normed,
            step_size_input,
            step_size_bias[layer_position],
            head_decay_logarithm[layer_position],
            direct_path_gain[layer_position],
        )
        states_new.append(updated_state)
        gated_out = readout_key_vector * jax.nn.silu(gate_in.astype(jnp.float32))
        normed = group_norm(gated_out, output_norm_gain[layer_position], group_width)
        out_weight = output_projection[layer_position]
        partial_value = jnp.dot(
            gather_directly(normed, "dp", 0), out_weight, preferred_element_type=jnp.float32
        )
        update_rows = sum_at_owner(partial_value, "tp", 0)
        own_rows = lax.dynamic_slice_in_dim(hidden_float, row_start, row_count, 0)
        hidden_rows = (own_rows + update_rows).astype(jnp.bfloat16)
        if layer_position + 1 < LAYERS:
            hidden_cols = gather_directly(hidden_rows, "tp", 0)
    return (hidden_rows, jnp.stack(states_new), jnp.stack(windows_new))


def solution(mesh):
    placed = (
        P("grp", "dp"),
        P(("grp", "dp")),
        P(None, "dp"),
        P(None, "dp", "tp"),
        P(None, "dp", "tp"),
        P(None, "dp", "tp"),
        P(None, "dp", "tp"),
        P(None, "dp", None),
        P(None, None, None, "tp"),
        P(None, ("grp", "dp"), None, None, "tp"),
        P(None, "tp"),
        P(None, "tp"),
        P(None, "tp"),
        P(None, ("grp", "dp"), "tp"),
        P(None, ("grp", "dp"), "tp", None, None),
        P(None, "tp"),
        P(None, "tp", "dp"),
    )
    return jax.shard_map(
        body,
        mesh=mesh,
        in_specs=placed,
        out_specs=(
            P(("grp", "tp"), "dp"),
            P(None, ("grp", "dp"), "tp", None, None),
            P(None, ("grp", "dp"), None, None, "tp"),
        ),
        check_vma=False,
    )
```

profile of v0, /device:TPU:40, one launch (start us, length us, event | category | flops | bytes accessed | tf_op | source)
XLA Modules:
  0.0 190.6 jit_solution(15587935974363407212)
XLA Ops:
  0.6 0.8 fusion.97
  1.4 1.0 multiply_reduce_fusion.1
  2.4 1.1 fusion.34
  3.5 1.1 fusion.32
  4.6 0.2 fusion.30
  4.8 0.2 fusion.28
  5.0 0.1 concatenate.24
  5.1 0.1 fusion.81
  5.3 0.7 concatenate.19
  6.0 4.7 %all-to-all-start = ((f32[8,8,515]{2,1,0:T(8,128)}), f32[8,8,515]{2,1,0:T(8,128)S(1)}, u32[]{:S(2)}, u32[]{:S(2)}) async-start(f32[8,8,515]{2,1,0:T(8,128)} %concatenate.19), calls=%async_computation | async-start | bytes 327680 | tf_op jit(solution)/shard_map/all_to_all | solution.py:25
  10.9 0.6 copy-done.10
  11.4 0.1 copy.84
  11.6 0.6 copy-done.15
  12.2 0.1 compare_convert_fusion
  12.3 0.6 copy-done.13
  12.9 0.2 multiply_reduce_fusion.3
  13.1 4.1 %all-to-all-done = f32[8,8,515]{2,1,0:T(8,128)S(1)} async-done(((f32[8,8,515]{2,1,0:T(8,128)}), f32[8,8,515]{2,1,0:T(8,128)S(1)}, u32[]{:S(2)}, u32[]{:S(2)}) %all-to-all-start) | async-done | bytes 131872 | tf_op jit(solution)/shard_map/all_to_all | solution.py:25
  17.2 0.2 fusion.72
  17.4 0.1 fusion.73
  17.5 0.1 reshape_squeeze.13
  17.6 0.1 add_exponential_fusion.1
  17.7 0.1 broadcast_multiply_fusion.1
  17.8 0.4 fusion.4
  18.2 0.1 multiply_add_fusion.3
  18.3 0.1 reshape.273
  18.3 0.2 multiply_reduce_fusion.5
  18.6 0.1 multiply_convert_fusion.3
  18.6 7.8 %all_to_all.35 = bf16[8,8,128]{2,1,0:T(8,128)(2,1)S(1)} all-to-all(bf16[8,8,128]{2,1,0:T(8,128)(2,1)S(1)} %broadcast_in_dim.10), channel_id=1, replica_groups=mesh['grp'=2,'tp'=32,'dp'=8] {'dp'}, dimensions={0} | all-to-all | bytes 32768 | tf_op jit(solution)/shard_map/all_to_all | solution.py:43
  26.4 0.1 fusion.26
  26.6 0.8 copy.88
  27.3 45.8 %all-to-all-start.2 = ((f32[32,2,512]{2,1,0:T(2,128)}), f32[32,2,512]{2,1,0:T(2,128)S(1)}, u32[]{:S(2)}, u32[]{:S(2)}) async-start(f32[32,2,512]{2,1,0:T(2,128)} %copy.88), calls=%async_computation.2 | async-start | bytes 262144 | tf_op jit(solution)/shard_map/all_to_all | solution.py:25
  73.1 30.8 %all-to-all-done.2 = f32[32,2,512]{2,1,0:T(2,128)S(1)} async-done(((f32[32,2,512]{2,1,0:T(2,128)}), f32[32,2,512]{2,1,0:T(2,128)S(1)}, u32[]{:S(2)}, u32[]{:S(2)}) %all-to-all-start.2) | async-done | bytes 131104 | tf_op jit(solution)/shard_map/all_to_all | solution.py:25
  104.0 27.8 %all_to_all.36 = bf16[32,2,512]{2,1,0:T(2,128)(2,1)S(1)} all-to-all(bf16[32,2,512]{2,1,0:T(2,128)(2,1)S(1)} %broadcast_in_dim.11), channel_id=1, replica_groups=mesh['grp'=2,'tp'=32,'dp'=8] {'tp'}, dimensions={0} | all-to-all | bytes 131072 | tf_op jit(solution)/shard_map/all_to_all | solution.py:43
  131.8 0.2 multiply_reduce_fusion
  132.0 0.2 fusion.24
  132.2 0.6 copy-done.3
  132.8 0.2 fusion.22
  132.9 0.2 fusion.20
  133.1 0.2 fusion.18
  133.2 0.1 fusion.79
  133.4 0.1 concatenate.25
  133.4 0.8 concatenate.21
  134.2 3.6 %all-to-all-start.4 = ((f32[8,8,515]{2,1,0:T(8,128)}), f32[8,8,515]{2,1,0:T(8,128)S(1)}, u32[]{:S(2)}, u32[]{:S(2)}) async-start(f32[8,8,515]{2,1,0:T(8,128)} %concatenate.21), calls=%async_computation.4 | async-start | bytes 327680 | tf_op jit(solution)/shard_map/all_to_all | solution.py:25
  137.8 0.1 copy.91
  137.9 6.1 %all-to-all-done.4 = f32[8,8,515]{2,1,0:T(8,128)S(1)} async-done(((f32[8,8,515]{2,1,0:T(8,128)}), f32[8,8,515]{2,1,0:T(8,128)S(1)}, u32[]{:S(2)}, u32[]{:S(2)}) %all-to-all-start.4) | async-done | bytes 131872 | tf_op jit(solution)/shard_map/all_to_all | solution.py:25
  144.1 0.2 fusion.64
  144.2 0.1 fusion.76
  144.4 0.1 reshape_squeeze.15
  144.5 0.1 add_exponential_fusion
  144.5 0.1 broadcast_multiply_fusion
  144.6 0.4 fusion.1
  145.0 0.1 multiply_add_fusion.2
  145.1 0.1 reshape.275
  145.2 0.2 multiply_reduce_fusion.4
  145.4 0.1 multiply_convert_fusion.2
  145.5 7.8 %all_to_all.37 = bf16[8,8,128]{2,1,0:T(8,128)(2,1)S(1)} all-to-all(bf16[8,8,128]{2,1,0:T(8,128)(2,1)S(1)} %broadcast_in_dim.12), channel_id=1, replica_groups=mesh['grp'=2,'tp'=32,'dp'=8] {'dp'}, dimensions={0} | all-to-all | bytes 32768 | tf_op jit(solution)/shard_map/all_to_all | solution.py:43
  153.3 0.1 fusion.16
  153.4 0.8 copy.95
  154.2 4.8 %all-to-all-start.6 = ((f32[32,2,512]{2,1,0:T(2,128)}), f32[32,2,512]{2,1,0:T(2,128)S(1)}, u32[]{:S(2)}, u32[]{:S(2)}) async-start(f32[32,2,512]{2,1,0:T(2,128)} %copy.95), calls=%async_computation.6 | async-start | bytes 262144 | tf_op jit(solution)/shard_map/all_to_all | solution.py:25
  159.2 0.7 pad_maximum_fusion.1
  159.8 0.4 multiply_add_fusion.1
  160.2 1.0 pad_maximum_fusion
  161.3 28.7 %all-to-all-done.6 = f32[32,2,512]{2,1,0:T(2,128)S(1)} async-done(((f32[32,2,512]{2,1,0:T(2,128)}), f32[32,2,512]{2,1,0:T(2,128)S(1)}, u32[]{:S(2)}, u32[]{:S(2)}) %all-to-all-start.6) | async-done | bytes 131104 | tf_op jit(solution)/shard_map/all_to_all | solution.py:25
  190.0 0.6 add_convert_fusion
  (68 shorter events, 0.7 us)
Async XLA Ops:
  0.6 1.8 copy-start
  1.4 3.2 %copy-start.4 = (bf16[2,512,128]{2,1,0:T(8,128)(2,1)S(1)}, bf16[2,512,128]{2,1,0:T(8,128)(2,1)}, u32[]{:S(2)}) copy-start(bf16[2,512,128]{2,1,0:T(8,128)(2,1)} %param.22) | copy-start | bytes 786436
  3.5 1.3 copy-start.5
  3.5 1.5 copy-start.8
  4.6 13.2 %copy-start.1 = (f32[2,8,2,64,128]{4,3,2,1,0:T(8,128)S(1)}, f32[2,8,2,64,128]{4,3,2,1,0:T(8,128)}, u32[]{:S(2)}) copy-start(f32[2,8,2,64,128]{4,3,2,1,0:T(8,128)} %param.31) | copy-start | bytes 3145732
  6.0 4.7 %copy-start.9 = (bf16[2,5,3,128]{3,0,2,1:T(2,128)(2,1)S(1)}, bf16[2,5,3,128]{3,0,2,1:T(2,128)(2,1)}, u32[]{:S(2)}) copy-start(bf16[2,5,3,128]{3,0,2,1:T(2,128)(2,1)} %param.25) | copy-start | bytes 23044
  6.0 11.2 %all-to-all-start = ((f32[8,8,515]{2,1,0:T(8,128)}), f32[8,8,515]{2,1,0:T(8,128)S(1)}, u32[]{:S(2)}, u32[]{:S(2)}) async-start(f32[8,8,515]{2,1,0:T(8,128)} %concatenate.19), calls=%async_computation | async-start | bytes 327680 | tf_op jit(solution)/shard_map/all_to_all | solution.py:25
  10.8 0.7 copy-start.10
  10.8 0.8 copy-start.11
  10.8 0.8 copy-start.12
  10.8 2.1 %copy-start.7 = (bf16[2,8,4,3,128]{4,2,3,1,0:T(4,128)(2,1)S(1)}, bf16[2,8,4,3,128]{4,2,3,1,0:T(4,128)(2,1)}, u32[]{:S(2)}) copy-start(bf16[2,8,4,3,128]{4,2,3,1,0:T(4,128)(2,1)} %param.26) | copy-start | bytes 147460
  11.5 0.7 copy-start.15
  12.2 0.7 copy-start.13
  12.2 0.7 copy-start.14
  17.8 8.6 %copy-start.6 = (bf16[2,128,512]{2,1,0:T(8,128)(2,1)S(1)}, bf16[2,128,512]{2,1,0:T(8,128)(2,1)}, u32[]{:S(2)}) copy-start(bf16[2,128,512]{2,1,0:T(8,128)(2,1)} %param.33) | copy-start | bytes 786436
  27.3 76.6 %all-to-all-start.2 = ((f32[32,2,512]{2,1,0:T(2,128)}), f32[32,2,512]{2,1,0:T(2,128)S(1)}, u32[]{:S(2)}, u32[]{:S(2)}) async-start(f32[32,2,512]{2,1,0:T(2,128)} %copy.88), calls=%async_computation.2 | async-start | bytes 262144 | tf_op jit(solution)/shard_map/all_to_all | solution.py:25
  104.0 28.0 %copy-start.2 = (bf16[2,512,128]{2,1,0:T(8,128)(2,1)S(1)}, bf16[2,512,128]{2,1,0:T(8,128)(2,1)}, u32[]{:S(2)}) copy-start(bf16[2,512,128]{2,1,0:T(8,128)(2,1)} %param.20) | copy-start | bytes 786436
  131.8 1.0 copy-start.3
  134.2 9.8 %all-to-all-start.4 = ((f32[8,8,515]{2,1,0:T(8,128)}), f32[8,8,515]{2,1,0:T(8,128)S(1)}, u32[]{:S(2)}, u32[]{:S(2)}) async-start(f32[8,8,515]{2,1,0:T(8,128)} %concatenate.21), calls=%async_computation.4 | async-start | bytes 327680 | tf_op jit(solution)/shard_map/all_to_all | solution.py:25
  154.2 35.8 %all-to-all-start.6 = ((f32[32,2,512]{2,1,0:T(2,128)}), f32[32,2,512]{2,1,0:T(2,128)S(1)}, u32[]{:S(2)}, u32[]{:S(2)}) async-start(f32[32,2,512]{2,1,0:T(2,128)} %copy.95), calls=%async_computation.6 | async-start | bytes 262144 | tf_op jit(solution)/shard_map/all_to_all | solution.py:25
where the time goes:
time: 191 us
  waiting for transfers between devices  69.7 us (36%)
  starting transfers between devices  58.8 us (31%)
  blocking collectives  43.3 us (23%)
  local copies, waits for them, and re-layouts  7.22 us (4%)
  other arithmetic  5.97 us (3%)
  matrix products  4.46 us (2%)
    all_to_all x4, waiting for transfers between devices, sum_at_owner(): lax.all_to_all(blocks, axis, split_axis=0, concat_axis=0, tiled=True)  69.7 us
    all_to_all x4, starting transfers between devices, sum_at_owner(): lax.all_to_all(blocks, axis, split_axis=0, concat_axis=0, tiled=True)  58.8 us
    all_to_all x3, blocking collectives, copy_for_each(): lax.all_to_all(jnp.broadcast_to(shard[None], (devices, *shard.shape)), ax...  43.3 us
  transfers between devices with their start and end apart: 4, of which 4 were waited for; matrix products, arithmetic and copies ran while one was open for 1% of the time, Pallas kernels for 0%

commit v1 on v0

v1 whole, which is shorter than its diff:
```python
import functools

import jax
import jax.numpy as jnp
from jax import lax
from jax.experimental import pallas as pl
from jax.experimental.pallas import tpu as pltpu
from jax.sharding import PartitionSpec as P

D = 4096
EPSILON = 1e-06
MESH = pl.DeviceIdType.MESH
F32 = jnp.float32
BF16 = jnp.bfloat16
REACH = 4
STAT = 3


def total_wait(buffer, count, sem):
    part = buffer.at[pl.ds(0, count)]
    pltpu.make_async_copy(part, part, sem).wait()


def kernel(
    n_tp,
    n_dp,
    h_in,
    counts,
    in_gain,
    w_value,
    w_inkey,
    w_readkey,
    w_gate,
    w_step,
    taps,
    history,
    step_bias,
    decay_log,
    direct_gain,
    extra_log,
    state_in,
    out_gain,
    w_out,
    hidden_out,
    state_out,
    window_out,
    h_v,
    wp_v,
    ws_v,
    wo_v,
    hist_v,
    state_v,
    hist_f,
    early_v,
    cur_f,
    normed_f,
    tile_f,
    res_f,
    in_send,
    in_recv,
    mix_send,
    mix_recv,
    part_send,
    part_recv,
    own_send,
    own_recv,
    load_sem,
    state_sem,
    send_sem,
    recv_sem,
    far_sem,
):
    layers = w_out.shape[0]
    batch, feats = h_in.shape
    rows = batch // n_dp
    chans = w_out.shape[1]
    blocks = feats // 128
    head_dim = state_in.shape[3]
    heads = state_in.shape[2]
    width_back = history.shape[2]
    me_tp = lax.axis_index("tp")
    me_dp = lax.axis_index("dp")

    def tp_at(shift):
        return {"tp": lax.rem(me_tp + (n_tp + shift), n_tp)}

    def dp_at(shift):
        return {"dp": lax.rem(me_dp + shift, n_dp)}

    barrier = pltpu.get_barrier_semaphore()
    for shift in range(1, n_dp):
        pl.semaphore_signal(barrier, inc=1, device_id=dp_at(shift), device_id_type=MESH)
    for shift in range(1, REACH + 1):
        for to in (shift, -shift):
            pl.semaphore_signal(barrier, inc=1, device_id=tp_at(to), device_id_type=MESH)

    loads = [pltpu.make_async_copy(h_in, h_v, load_sem.at[0])]
    for l in range(layers):
        for k, w in enumerate((w_value, w_inkey, w_readkey, w_gate)):
            loads.append(pltpu.make_async_copy(w.at[l], wp_v.at[l, k], load_sem.at[1 + l]))
        loads.append(pltpu.make_async_copy(w_step.at[l], ws_v.at[l], load_sem.at[1 + l]))
        if l == 0:
            loads.append(pltpu.make_async_copy(history, hist_v, load_sem.at[3]))
            loads.append(pltpu.make_async_copy(state_in.at[0], state_v.at[0], load_sem.at[4]))
            loads.append(pltpu.make_async_copy(w_out.at[0], wo_v.at[0], load_sem.at[5]))
        else:
            loads.append(pltpu.make_async_copy(state_in.at[l], state_v.at[l], load_sem.at[6]))
            loads.append(pltpu.make_async_copy(w_out.at[l], wo_v.at[l], load_sem.at[7]))
    for load in loads:
        load.start()

    lane = lax.broadcasted_iota(jnp.int32, (rows, 128), 1)
    lane_all = lax.broadcasted_iota(jnp.int32, (batch, 128), 1)
    sub = lax.broadcasted_iota(jnp.int32, (rows, 128), 0)
    first_head = lane < head_dim

    def spread(values, in_layer):
        return jnp.where(first_head, values[in_layer, 0], values[in_layer, 1])

    def project(l, h):
        squares = jnp.sum(h * h, axis=1, keepdims=True)
        scaled = (h * in_gain[l : l + 1, :]).astype(BF16)
        for k in range(4):
            part = jnp.dot(scaled, wp_v[l, k], preferred_element_type=F32)
            for i in range(n_dp):
                in_send[l, i, k] = part[i * rows : (i + 1) * rows].astype(BF16)
        steps = jnp.dot(scaled, ws_v[l], preferred_element_type=F32)
        lane_step = lax.broadcasted_iota(jnp.int32, steps.shape, 1)
        wanted = [
            jnp.sum(jnp.where(lane_step == me_tp * heads + k, steps, 0.0), axis=1, keepdims=True)
            for k in range(heads)
        ] + [squares]
        stats = jnp.zeros((batch, 128), F32)
        for k, v in enumerate(wanted):
            high = v.astype(BF16).astype(F32)
            stats = jnp.where(lane_all == k, high, stats)
            stats = jnp.where(lane_all == k + STAT, v - high, stats)
        for i in range(n_dp):
            in_send[l, i, 4] = stats[i * rows : (i + 1) * rows].astype(BF16)
        in_recv[l, me_dp] = in_send[l, me_dp]

    def send_in(l):
        for shift in range(1, n_dp):
            to = dp_at(shift)
            pltpu.make_async_remote_copy(
                src_ref=in_send.at[l, to["dp"]],
                dst_ref=in_recv.at[l, me_dp],
                send_sem=send_sem.at[l],
                recv_sem=recv_sem.at[l],
                device_id=to,
                device_id_type=MESH,
            ).start()

    def earlier(l):
        lens = jnp.zeros((rows, 128), jnp.int32)
        for b in range(rows):
            lens = jnp.where(sub == b, counts[b], lens)
        for b in range(rows):
            for j in range(width_back):
                hist_f[pl.ds((b * width_back + j) * 4, 3), :] = hist_v[l, b, j].astype(F32)
        weights = taps[l].astype(F32)
        for r in range(3):
            total = jnp.zeros((rows, 128), F32)
            for j in range(width_back):
                past = hist_f[pl.ds(j * 4 + r, rows, stride=4 * width_back), :]
                live = jnp.where(lens >= width_back - j, past, 0.0)
                total = total + live * weights[j, r : r + 1]
            early_v[l, r] = total + 0.0
        for b in range(rows):
            for j in range(1, width_back):
                window_out[l, b, j - 1] = hist_v[l, b, j]

    def mixer(l):
        arrived = jnp.sum(in_recv[l].astype(F32), axis=0)
        stats = arrived[4]

        def stat(k):
            both = jnp.where((lane == k) | (lane == k + STAT), stats, 0.0)
            return jnp.sum(both, axis=1, keepdims=True)

        inverse = lax.rsqrt(stat(heads) / D + EPSILON)
        current = [(inverse * arrived[k]).astype(BF16).astype(F32) for k in range(3)]
        gate = (inverse * arrived[3]).astype(BF16).astype(F32)
        step = jnp.where(first_head, stat(0), stat(1)) * inverse
        step = step.astype(BF16).astype(F32)
        weights = taps[l].astype(F32)
        mixed = [
            jax.nn.silu(early_v[l, r] + current[r] * weights[width_back, r : r + 1])
            for r in range(3)
        ]
        value, inkey, readkey = mixed
        rate = jax.nn.softplus(step + spread(step_bias, l))
        extra = jnp.where(first_head, extra_log[l, :, 0:1], extra_log[l, :, 1:2])
        decay = jnp.exp(-rate * jnp.exp(spread(decay_log, l)) + extra)
        gain = rate * value
        gain_t = jnp.transpose(jnp.concatenate([gain] * (128 // rows), axis=0))
        lane_sq = lax.broadcasted_iota(jnp.int32, (head_dim, 128), 1)
        reads = [jnp.zeros((head_dim, 128), F32) for _ in range(heads)]
        for b in range(rows):
            key_b = jnp.broadcast_to(inkey[b : b + 1], (head_dim, 128))
            read_b = jnp.broadcast_to(readkey[b : b + 1], (head_dim, 128))
            for k in range(heads):
                decay_b = decay[b : b + 1, k * head_dim : k * head_dim + 1]
                column = gain_t[k * head_dim : (k + 1) * head_dim, b : b + 1]
                new = decay_b * state_v[l, b, k] + column * key_b
                state_v[l, b, k] = new
                read = jnp.sum(new * read_b, axis=1, keepdims=True)
                reads[k] = jnp.where(lane_sq == b, read, reads[k])
        pltpu.make_async_copy(state_v.at[l], state_out.at[l], state_sem).start()
        readout = jnp.transpose(jnp.concatenate(reads, axis=0))[0:rows]
        readout = readout + spread(direct_gain, l) * value
        gated = readout * jax.nn.silu(gate)
        scale = lax.rsqrt(jnp.mean(gated * gated, axis=1, keepdims=True) + EPSILON)
        normed = (gated * scale * out_gain[l : l + 1, :]).astype(BF16)
        mix_send[l] = normed
        mix_recv[l, me_dp] = normed
        for r in range(3):
            cur_f[pl.ds(r, rows, stride=4), :] = current[r]
        for b in range(rows):
            window_out[l, b, width_back - 1] = cur_f[pl.ds(4 * b, 3), :].astype(BF16)

    def send_mix(l):
        for shift in range(1, n_dp):
            pltpu.make_async_remote_copy(
                src_ref=mix_send.at[l],
                dst_ref=mix_recv.at[l, me_dp],
                send_sem=send_sem.at[layers + l],
                recv_sem=recv_sem.at[layers + l],
                device_id=dp_at(shift),
                device_id_type=MESH,
            ).start()

    def ring_send(source, target, sem):
        def pair(step, _):
            shift = n_tp // 2 - step

            def to(shift):
                at = lax.rem(me_tp + shift, n_tp)
                pltpu.make_async_remote_copy(
                    src_ref=source(at),
                    dst_ref=target,
                    send_sem=send_sem.at[sem],
                    recv_sem=recv_sem.at[sem],
                    device_id={"tp": at},
                    device_id_type=MESH,
                ).start()

            to(shift)
            to(n_tp - shift)
            return 0

        at_far = lax.rem(me_tp + n_tp // 2, n_tp)
        pltpu.make_async_remote_copy(
            src_ref=source(at_far),
            dst_ref=target,
            send_sem=send_sem.at[sem],
            recv_sem=recv_sem.at[sem],
            device_id={"tp": at_far},
            device_id_type=MESH,
        ).start()
        lax.fori_loop(1, n_tp // 2, pair, 0)

    loads[0].wait()
    h = h_v[...].astype(F32)
    for i in range(n_dp):
        for j in range(blocks):
            res_f[i * blocks + j] = h[i * rows : (i + 1) * rows, j * 128 : (j + 1) * 128]
    for load in loads[1:6]:
        load.wait()
    project(0, h)
    pl.semaphore_wait(barrier, n_dp - 1 + 2 * REACH)
    for to in (REACH, -REACH):
        pl.semaphore_signal(far_sem.at[0], inc=1, device_id=tp_at(to), device_id_type=MESH)
    send_in(0)
    loads[6].wait()
    earlier(0)
    earlier(1)
    loads[7].wait()

    for l in range(layers):
        total_wait(in_recv.at[l], n_dp - 1, recv_sem.at[l])
        mixer(l)
        if l == 0:
            pl.semaphore_wait(far_sem.at[0], 2)
            for to in (2 * REACH, -2 * REACH):
                pl.semaphore_signal(
                    far_sem.at[1], inc=1, device_id=tp_at(to), device_id_type=MESH
                )
        send_mix(l)
        loads[8 if l == 0 else 15].wait()
        total_wait(mix_recv.at[l], n_dp - 1, recv_sem.at[layers + l])
        if l + 1 < layers:
            mix = jnp.concatenate(
                [mix_recv[l, i].astype(F32) for i in range(n_dp)], axis=0
            ).astype(BF16)
            part = jnp.dot(mix, wo_v[l], preferred_element_type=F32)
            for i in range(n_dp):
                for j in range(blocks):
                    part_send[l, i * blocks + j] = part[
                        i * rows : (i + 1) * rows, j * 128 : (j + 1) * 128
                    ].astype(BF16)
            part_recv[l, me_tp] = part_send[l, me_tp]
            pl.semaphore_wait(far_sem.at[1], 2)
            ring_send(lambda at: part_send.at[l, at], part_recv.at[l, me_tp], 2 * layers + l)
            total_wait(part_recv.at[l], n_tp - 1, recv_sem.at[2 * layers + l])
            mine = jnp.sum(part_recv[l].astype(F32), axis=0) + res_f[me_tp]
            own_send[...] = mine.astype(BF16)
            own_recv[me_tp] = mine.astype(BF16)
            ring_send(lambda at: own_send, own_recv.at[me_tp], 3 * layers)
            for load in loads[9:15]:
                load.wait()
            total_wait(own_recv, n_tp - 1, recv_sem.at[3 * layers])
            h = jnp.concatenate(
                [
                    jnp.concatenate(
                        [own_recv[i * blocks + j].astype(F32) for j in range(blocks)], axis=1
                    )
                    for i in range(n_dp)
                ],
                axis=0,
            )
            project(l + 1, h)
            send_in(l + 1)
            h_v[...] = h.astype(BF16)
        else:
            for i in range(n_dp):
                normed_f[i * rows : (i + 1) * rows, :] = mix_recv[l, i].astype(F32)
            mix = jnp.concatenate(
                [normed_f[pl.ds(r, batch // 2, stride=2), :] for r in range(2)], axis=0
            ).astype(BF16)
            part = jnp.dot(mix, wo_v[l], preferred_element_type=F32)
            for j in range(blocks):
                for r in range(2):
                    tile_f[pl.ds(2 * j + r, n_tp, stride=8), :] = part[
                        r * n_tp : (r + 1) * n_tp, j * 128 : (j + 1) * 128
                    ]
            for i in range(n_tp):
                part_send[l, i] = tile_f[i * 8 : (i + 1) * 8, :].astype(BF16)
            part_recv[l, me_tp] = part_send[l, me_tp]
            ring_send(lambda at: part_send.at[l, at], part_recv.at[l, me_tp], 2 * layers + l)
            at_row = lax.broadcasted_iota(jnp.int32, (8, batch), 0)
            at_col = lax.broadcasted_iota(jnp.int32, (8, batch), 1)
            pick = ((at_col == 2 * me_tp + at_row) & (at_row < 2)).astype(BF16)
            kept = jnp.dot(pick, h_v[...], preferred_element_type=F32)[0:2]
            total_wait(part_recv.at[l], n_tp - 1, recv_sem.at[2 * layers + l])
            tile = jnp.sum(part_recv[l].astype(F32), axis=0)
            update = jnp.concatenate([tile[2 * j : 2 * j + 2] for j in range(blocks)], axis=1)
            hidden_out[...] = (kept + update).astype(BF16)

    for l in range(layers):
        total_wait(in_send.at[l], n_dp - 1, send_sem.at[l])
        for _ in range(n_dp - 1):
            pltpu.make_async_copy(mix_send.at[l], mix_send.at[l], send_sem.at[layers + l]).wait()
        total_wait(part_send.at[l], n_tp - 1, send_sem.at[2 * layers + l])
        pltpu.make_async_copy(state_v.at[l], state_out.at[l], state_sem).wait()
    total_wait(own_recv, n_tp - 1, send_sem.at[3 * layers])


def body(n_tp, n_dp, *args):
    h, _, _, w_value = args[:4]
    w_step, history, state, w_out = args[7], args[9], args[14], args[16]
    layers, feats, chans = w_value.shape
    batch = h.shape[0]
    rows = batch // n_dp
    vmem = pl.BlockSpec(memory_space=pltpu.VMEM)
    smem = pl.BlockSpec(memory_space=pltpu.SMEM)
    hbm = pl.BlockSpec(memory_space=pl.ANY)
    in_specs = [
        hbm, smem, vmem, hbm, hbm, hbm, hbm, hbm, vmem, hbm, smem, smem, smem, vmem, hbm, vmem, hbm,
    ]
    return pl.pallas_call(
        functools.partial(kernel, n_tp, n_dp),
        out_shape=(
            jax.ShapeDtypeStruct((batch // n_tp, feats), BF16),
            jax.ShapeDtypeStruct(state.shape, F32),
            jax.ShapeDtypeStruct(history.shape, BF16),
        ),
        in_specs=in_specs,
        out_specs=(vmem, hbm, vmem),
        scratch_shapes=[
            pltpu.VMEM((batch, feats), BF16),
            pltpu.VMEM((layers, 4, feats, chans), BF16),
            pltpu.VMEM(w_step.shape, BF16),
            pltpu.VMEM(w_out.shape, BF16),
            pltpu.VMEM(history.shape, BF16),
            pltpu.VMEM(state.shape, F32),
            pltpu.VMEM((rows * 16, 128), F32),
            pltpu.VMEM((layers, 3, rows, 128), F32),
            pltpu.VMEM((rows * 4, 128), F32),
            pltpu.VMEM((batch, 128), F32),
            pltpu.VMEM((n_tp * 8, 128), F32),
            pltpu.VMEM((n_tp, 8, 128), F32),
            pltpu.VMEM((layers, n_dp, 5, rows, 128), BF16),
            pltpu.VMEM((layers, n_dp, 5, rows, 128), BF16),
            pltpu.VMEM((layers, rows, 128), BF16),
            pltpu.VMEM((layers, n_dp, rows, 128), BF16),
            pltpu.VMEM((layers, n_tp, 8, 128), BF16),
            pltpu.VMEM((layers, n_tp, 8, 128), BF16),
            pltpu.VMEM((8, 128), BF16),
            pltpu.VMEM((n_tp, 8, 128), BF16),
            pltpu.SemaphoreType.DMA((8,)),
            pltpu.SemaphoreType.DMA,
            pltpu.SemaphoreType.DMA((3 * layers + 1,)),
            pltpu.SemaphoreType.DMA((3 * layers + 1,)),
            pltpu.SemaphoreType.REGULAR((2,)),
        ],
        compiler_params=pltpu.CompilerParams(collective_id=0, has_side_effects=True),
    )(*args)


def solution(mesh):
    placed = (
        P("grp", "dp"),
        P(("grp", "dp")),
        P(None, "dp"),
        P(None, "dp", "tp"),
        P(None, "dp", "tp"),
        P(None, "dp", "tp"),
        P(None, "dp", "tp"),
        P(None, "dp", None),
        P(None, None, None, "tp"),
        P(None, ("grp", "dp"), None, None, "tp"),
        P(None, "tp"),
        P(None, "tp"),
        P(None, "tp"),
        P(None, ("grp", "dp"), "tp"),
        P(None, ("grp", "dp"), "tp", None, None),
        P(None, "tp"),
        P(None, "tp", "dp"),
    )
    return jax.shard_map(
        functools.partial(body, mesh.shape["tp"], mesh.shape["dp"]),
        mesh=mesh,
        in_specs=placed,
        out_specs=(
            P(("grp", "tp"), "dp"),
            P(None, ("grp", "dp"), "tp", None, None),
            P(None, ("grp", "dp"), None, None, "tp"),
        ),
        check_vma=False,
    )
```

time: 191 us -> 115 us (0.60)
  Pallas kernels: 0 us -> 106 us
  waiting for transfers between devices: 69.7 us -> 0 us
  starting transfers between devices: 58.8 us -> 0 us
  blocking collectives: 43.3 us -> 0 us
  other arithmetic: 5.97 us -> 0 us
  matrix products: 4.46 us -> 0 us
    pallas_call x0 -> x1, Pallas kernels: none -> 106 us  [body(): pl.pallas_call(functools.partial(kernel, n_tp, n_dp), out_shape=(jax.Shap...]
    all_to_all x4 -> x0, waiting for transfers between devices: 69.7 us -> none  [sum_at_owner(): lax.all_to_all(blocks, axis, split_axis=0, concat_axis=0, tiled=True)]
    all_to_all x4 -> x0, starting transfers between devices: 58.8 us -> none  [sum_at_owner(): lax.all_to_all(blocks, axis, split_axis=0, concat_axis=0, tiled=True)]
    all_to_all x3 -> x0, blocking collectives: 43.3 us -> none  [copy_for_each(): lax.all_to_all(jnp.broadcast_to(shard[None], (devices, *shard.shape)), ax...]
    unnamed x34 -> x12, local copies, waits for them, and re-layouts: 2.47 us -> 7.17 us
    dot_general x14 -> x0, matrix products: 4.46 us -> none  [the longest x10 3.42 us: project_part(): return jnp.dot(scaled_in, weight, preferred_element_type=jnp.float32)]
    another operation x6 -> x0, other arithmetic: 1.92 us -> none  [the longest x4 1.76 us: body(): return (hidden_rows, jnp.stack(states_new), jnp.stack(windows_new))]
  transfers between devices with their start and end apart: 4 -> 0, of which waited for: 4 -> 0; matrix products, arithmetic and copies ran while one was open for 1% -> 0% of each run, Pallas kernels for 0% -> 0%
where the time goes in v1:
time: 115 us
  Pallas kernels  106 us (92%)
  local copies, waits for them, and re-layouts  8.65 us (8%)
    pallas_call x1, Pallas kernels, body(): pl.pallas_call(functools.partial(kernel, n_tp, n_dp), out_shape=(jax.Shap...  106 us
    unnamed x12, local copies, waits for them, and re-layouts  7.17 us

profile of v1, /device:TPU:40, one launch (start us, length us, event | category | flops | bytes accessed | tf_op | source)
XLA Modules:
  0.0 115.0 jit_solution(17727034499512069901)
XLA Ops:
  0.6 0.0 copy-start.1
  0.6 0.0 copy-start
  0.7 1.4 %copy.23.extra_log = f32[2,8,2]{2,1,0:T(8,128)} copy(f32[2,8,2]{1,2,0:T(2,128)} %param.30) | data formatting | bytes 256 | tf_op args[13]
  2.0 0.0 copy-done.1
  2.0 0.6 copy.21.taps
  2.6 1.4 %copy.22.history = bf16[2,8,4,3,128]{4,3,2,1,0:T(4,128)(2,1)} copy(bf16[2,8,4,3,128]{4,2,3,1,0:T(4,128)(2,1)} %param.26) | data formatting | bytes 98304 | tf_op args[9]
  4.1 0.0 copy-done
  4.1 0.8 copy.20.w_step
  4.9 105.7 %shard_map.184 = (bf16[2,512]{1,0:T(2,128)(2,1)}, f32[2,8,2,64,128]{4,3,2,1,0:T(8,128)}, bf16[2,8,4,3,128]{4,3,2,1,0:T(4,128)(2,1)}) custom-call(bf16[64,512]{1,0:T(8,128)(2,1)} %h_in.1, s32[8]{0:T(128)} %counts.1, f32[2,512]{1,0:T(2,128)} %in_gain.1, bf16[2,512,128]{2,1,0:T(8,128)(2,1)} %w_value.1, bf16[2,512,128]{2,1,0:T(8,128)(2,1)} %w_inkey.1, ...), custom_call_target="tpu_custom_call" | custom-call | tf_op jit(solution)/shard_map/pallas_call | solution.py:371
  110.6 0.0 copy-start.2
  110.6 1.5 %copy.24 = bf16[2,8,4,3,128]{4,2,3,1,0:T(4,128)(2,1)} copy(bf16[2,8,4,3,128]{4,3,2,1,0:T(4,128)(2,1)} %get-tuple-element.5) | data formatting | bytes 98304 | tf_op jit(solution)/shard_map/pallas_call | solution.py:371
  112.1 0.0 copy-done.2
  112.1 0.6 copy.27
  112.7 2.3 %copy.28 = f32[2,8,2,64,128]{4,3,2,1,0:T(8,128)} copy(f32[2,8,2,64,128]{4,3,2,1,0:T(8,128)} %get-tuple-element.10) | data formatting | bytes 2097152
Async XLA Ops:
  0.6 1.4 %copy-start.1 = (bf16[2,5,3,128]{3,0,2,1:T(2,128)(2,1)S(1)}, bf16[2,5,3,128]{3,0,2,1:T(2,128)(2,1)}, u32[]{:S(2)}) copy-start(bf16[2,5,3,128]{3,0,2,1:T(2,128)(2,1)} %param.25) | copy-start | bytes 23044
  0.6 3.4 %copy-start = (bf16[2,512,64]{1,2,0:T(8,128)(2,1)S(1)}, bf16[2,512,64]{1,2,0:T(8,128)(2,1)}, u32[]{:S(2)}) copy-start(bf16[2,512,64]{1,2,0:T(8,128)(2,1)} %param.24) | copy-start | bytes 393220
  110.6 1.5 %copy-start.2 = (bf16[2,512]{1,0:T(2,128)(2,1)S(1)}, bf16[2,512]{1,0:T(2,128)(2,1)}, u32[]{:S(2)}) copy-start(bf16[2,512]{1,0:T(2,128)(2,1)} %get-tuple-element.9) | copy-start | bytes 6148

commit v2 on v1

v2 whole, which is shorter than its diff:
```python
import functools

import jax
import jax.numpy as jnp
from jax import lax
from jax.experimental import pallas as pl
from jax.experimental.pallas import tpu as pltpu
from jax.sharding import PartitionSpec as P

D = 4096
EPSILON = 1e-06
MESH = pl.DeviceIdType.MESH
F32 = jnp.float32
BF16 = jnp.bfloat16
LANES = 128
STAT = 3


def total_wait(buffer, count, sem):
    part = buffer.at[pl.ds(0, count)]
    pltpu.make_async_copy(part, part, sem).wait()


def kernel(
    n_tp,
    n_dp,
    h_in,
    counts,
    in_gain,
    w_value,
    w_inkey,
    w_readkey,
    w_gate,
    w_step,
    taps,
    history,
    step_bias,
    decay_log,
    direct_gain,
    extra_log,
    state_in,
    out_gain,
    w_out,
    hidden_out,
    state_out,
    window_out,
    h_v,
    wp_v,
    wo_v,
    hist_v,
    state_v,
    hist_f,
    win_f,
    early_v,
    normed_f,
    tile_f,
    in_send,
    in_recv,
    mix_send,
    mix_recv,
    near_send,
    near_recv,
    far_recv,
    own_recv,
    part_send,
    part_recv,
    load_sem,
    state_sem,
    send_sem,
    recv_sem,
    know_sem,
):
    layers = w_out.shape[0]
    batch, feats = h_in.shape
    rows = batch // n_dp
    blocks = feats // LANES
    head_dim = state_in.shape[3]
    heads = state_in.shape[2]
    roles, width_back = history.shape[2:4]
    far = n_tp // blocks
    me_tp = lax.axis_index("tp")
    me_dp = lax.axis_index("dp")
    me_block = me_tp // blocks
    me_quarter = lax.rem(me_tp, blocks)

    def tp_at(shift):
        return {"tp": lax.rem(me_tp + (n_tp + shift), n_tp)}

    def dp_at(shift):
        return {"dp": lax.rem(me_dp + shift, n_dp)}

    def near_at(shift):
        return {"tp": me_block * blocks + lax.rem(me_quarter + shift, blocks)}

    def remote(source, target, sem, to):
        pltpu.make_async_remote_copy(
            src_ref=source,
            dst_ref=target,
            send_sem=send_sem.at[sem],
            recv_sem=recv_sem.at[sem],
            device_id=to,
            device_id_type=MESH,
        ).start()

    def signal(sem, to):
        pl.semaphore_signal(sem, inc=1, device_id=to, device_id_type=MESH)

    in_at = lambda l: l
    mix_at = lambda l: layers + l
    near_sum, far_sum, near_all, ring_sum = (2 * layers + k for k in range(4))

    barrier = pltpu.get_barrier_semaphore()
    for shift in range(1, n_dp):
        signal(barrier, dp_at(shift))
    for shift in range(1, blocks + 1):
        for to in (shift, -shift):
            signal(barrier, tp_at(to))

    def load(source, target, sem):
        copy = pltpu.make_async_copy(source, target, load_sem.at[sem])
        copy.start()
        return copy

    h_load = load(h_in, h_v, 0)
    w_loads, state_loads, wo_loads = [], [], []
    for l in range(layers):
        w_loads.append(
            [
                load(w.at[l], wp_v.at[l, :, pl.ds(k * LANES, LANES)], 1 + l)
                for k, w in enumerate((w_value, w_inkey, w_readkey, w_gate))
            ]
        )
        if l == 0:
            hist_load = load(history, hist_v, 1 + layers)
        state_loads.append(load(state_in.at[l], state_v.at[l], 2 + layers + l))
        wo_loads.append(load(w_out.at[l], wo_v.at[l], 2 + 2 * layers + l))

    lane = lax.broadcasted_iota(jnp.int32, (rows, LANES), 1)
    lane_all = lax.broadcasted_iota(jnp.int32, (batch, LANES), 1)
    sub = lax.broadcasted_iota(jnp.int32, (rows, LANES), 0)
    first_head = lane < head_dim

    def spread(values, in_layer):
        return jnp.where(first_head, values[in_layer, 0], values[in_layer, 1])

    def project(l, h):
        with jax.named_scope(f"proj{l}"):
            squares = jnp.sum(h * h, axis=1, keepdims=True)
            scaled = (h * in_gain[l : l + 1, :]).astype(BF16)
            steps = lax.dot_general(
                scaled, w_step[l], (((1,), (1,)), ((), ())), preferred_element_type=F32
            )
            lane_step = lax.broadcasted_iota(jnp.int32, steps.shape, 1)
            wanted = [
                jnp.sum(
                    jnp.where(lane_step == me_tp * heads + k, steps, 0.0), axis=1, keepdims=True
                )
                for k in range(heads)
            ] + [squares]
            for load in w_loads[l]:
                load.wait()
            part = jnp.dot(scaled, wp_v[l], preferred_element_type=F32)
            stats = jnp.zeros((batch, LANES), F32)
            for k, v in enumerate(wanted):
                high = v.astype(BF16).astype(F32)
                stats = jnp.where(lane_all == k, high, stats)
                stats = jnp.where(lane_all == k + STAT, v - high, stats)
            for i in range(n_dp):
                at = slice(i * rows, (i + 1) * rows)
                for k in range(4):
                    in_send[l, i, k] = part[at, k * LANES : (k + 1) * LANES].astype(BF16)
                in_send[l, i, 4] = stats[at].astype(BF16)

    def send_in(l):
        for shift in range(1, n_dp):
            to = dp_at(shift)
            remote(in_send.at[l, to["dp"]], in_recv.at[l, me_dp], in_at(l), to)
        in_recv[l, me_dp] = in_send[l, me_dp]

    def earlier(l):
        lens = jnp.zeros((rows, LANES), jnp.int32)
        for b in range(rows):
            lens = jnp.where(sub == b, counts[b], lens)
        for b in range(rows):
            for r in range(roles):
                hist_f[pl.ds((b * roles + r) * width_back, width_back), :] = hist_v[
                    l, b, r
                ].astype(F32)
        for r in range(roles):
            total = jnp.zeros((rows, LANES), F32)
            for j in range(width_back):
                past = hist_f[pl.ds(r * width_back + j, rows, stride=roles * width_back), :]
                live = jnp.where(lens >= width_back - j, past, 0.0)
                total = total + live * taps[j, r, l : l + 1].astype(F32)
                if j:
                    win_f[
                        l, pl.ds(r * width_back + j - 1, rows, stride=roles * width_back), :
                    ] = past
            early_v[l, r] = total

    def window(l):
        for b in range(rows):
            for r in range(roles):
                window_out[l, b, r] = win_f[
                    l, pl.ds((b * roles + r) * width_back, width_back), :
                ].astype(BF16)

    def mixer(l):
        with jax.named_scope(f"mixer{l}"):
            arrived = jnp.sum(in_recv[l].astype(F32), axis=0)
            stats = arrived[4]

            def stat(k):
                both = jnp.where((lane == k) | (lane == k + STAT), stats, 0.0)
                return jnp.sum(both, axis=1, keepdims=True)

            inverse = lax.rsqrt(stat(heads) / D + EPSILON)
            current = [(inverse * arrived[k]).astype(BF16).astype(F32) for k in range(roles)]
            gate = (inverse * arrived[3]).astype(BF16).astype(F32)
            step = jnp.where(first_head, stat(0), stat(1)) * inverse
            step = step.astype(BF16).astype(F32)
            value, inkey, readkey = [
                jax.nn.silu(
                    early_v[l, r] + current[r] * taps[width_back, r, l : l + 1].astype(F32)
                )
                for r in range(roles)
            ]
            rate = jax.nn.softplus(step + spread(step_bias, l))
            diagonal = lax.broadcasted_iota(
                jnp.int32, (rows, rows), 0
            ) == lax.broadcasted_iota(jnp.int32, (rows, rows), 1)
            extra = [
                jnp.sum(
                    jnp.where(diagonal, extra_log[l, k : k + 1, :], 0.0), axis=1, keepdims=True
                )
                for k in range(heads)
            ]
            extra = jnp.where(first_head, extra[0], extra[1])
            decay = jnp.exp(-rate * jnp.exp(spread(decay_log, l)) + extra)
            gain = rate * value
            gain_t = jnp.transpose(jnp.concatenate([gain] * (LANES // rows), axis=0))
            lane_sq = lax.broadcasted_iota(jnp.int32, (head_dim, LANES), 1)
            reads = [jnp.zeros((head_dim, LANES), F32) for _ in range(heads)]
            for b in range(rows):
                key_b = jnp.broadcast_to(inkey[b : b + 1], (head_dim, LANES))
                read_b = jnp.broadcast_to(readkey[b : b + 1], (head_dim, LANES))
                for k in range(heads):
                    decay_b = decay[b : b + 1, k * head_dim : k * head_dim + 1]
                    column = gain_t[k * head_dim : (k + 1) * head_dim, b : b + 1]
                    new = decay_b * state_v[l, b, k] + column * key_b
                    state_v[l, b, k] = new
                    read = jnp.sum(new * read_b, axis=1, keepdims=True)
                    reads[k] = jnp.where(lane_sq == b, read, reads[k])
            readout = jnp.transpose(jnp.concatenate(reads, axis=0))[0:rows]
            readout = readout + spread(direct_gain, l) * value
            gated = readout * jax.nn.silu(gate)
            scale = lax.rsqrt(jnp.mean(gated * gated, axis=1, keepdims=True) + EPSILON)
            normed = (gated * scale * out_gain[l : l + 1, :]).astype(BF16)
            mix_send[l] = normed
            mix_recv[l, me_dp] = normed
            for r in range(roles):
                win_f[
                    l, pl.ds((r + 1) * width_back - 1, rows, stride=roles * width_back), :
                ] = current[r]

    def send_mix(l):
        for shift in range(1, n_dp):
            remote(mix_send.at[l], mix_recv.at[l, me_dp], mix_at(l), dp_at(shift))
        pltpu.make_async_copy(state_v.at[l], state_out.at[l], state_sem).start()

    def reduce_all(l):
        with jax.named_scope("near_sum"):
            mix = jnp.concatenate(
                [mix_recv[l, i].astype(F32) for i in range(n_dp)], axis=0
            ).astype(BF16)
            part = jnp.dot(mix, wo_v[l], preferred_element_type=F32)
            for j in range(blocks):
                near_send[j] = part[:, j * LANES : (j + 1) * LANES].astype(BF16)
            for shift in range(1, blocks):
                to = near_at(shift)
                quarter = lax.rem(me_quarter + shift, blocks)
                remote(near_send.at[quarter], near_recv.at[me_quarter], near_sum, to)
            near_recv[me_quarter] = near_send[me_quarter]
            h = h_v[:, pl.ds(pl.multiple_of(me_quarter * LANES, LANES), LANES)].astype(F32)
        with jax.named_scope("near_wait"):
            total_wait(near_recv, blocks - 1, recv_sem.at[near_sum])
        with jax.named_scope("far_send"):
            far_recv[me_block] = jnp.sum(near_recv[...].astype(F32), axis=0).astype(BF16)
            pl.semaphore_wait(know_sem.at[1], 2)
            for step in range(far // 2, 0, -1):
                for shift in sorted({step, far - step}):
                    to = tp_at(shift * blocks)
                    remote(far_recv.at[me_block], far_recv.at[me_block], far_sum, to)
        with jax.named_scope("far_wait"):
            for load in w_loads[l + 1]:
                pass
            total_wait(far_recv, far - 1, recv_sem.at[far_sum])
        with jax.named_scope("near_all"):
            mine = (h + jnp.sum(far_recv[...].astype(F32), axis=0)).astype(BF16)
            own_recv[me_quarter] = mine
            for shift in range(1, blocks):
                remote(own_recv.at[me_quarter], own_recv.at[me_quarter], near_all, near_at(shift))
        with jax.named_scope("near_all_wait"):
            total_wait(own_recv, blocks - 1, recv_sem.at[near_all])
        return jnp.concatenate([own_recv[j].astype(F32) for j in range(blocks)], axis=1)

    def reduce_rows(l):
        with jax.named_scope("ring_send"):
            for i in range(n_dp):
                normed_f[i * rows : (i + 1) * rows, :] = mix_recv[l, i].astype(F32)
            kept_rows = batch // n_tp
            mix = jnp.concatenate(
                [normed_f[pl.ds(r, n_tp, stride=kept_rows), :] for r in range(kept_rows)], axis=0
            ).astype(BF16)
            part = jnp.dot(mix, wo_v[l], preferred_element_type=F32)
            for j in range(blocks):
                for r in range(kept_rows):
                    tile_f[pl.ds(kept_rows * j + r, n_tp, stride=8), :] = part[
                        r * n_tp : (r + 1) * n_tp, j * LANES : (j + 1) * LANES
                    ]
            for i in range(n_tp):
                part_send[i] = tile_f[i * 8 : (i + 1) * 8, :].astype(BF16)

            def to(shift):
                at = lax.rem(me_tp + shift, n_tp)
                remote(part_send.at[at], part_recv.at[me_tp], ring_sum, {"tp": at})

            def pair(step, _):
                to(n_tp // 2 - step)
                to(n_tp // 2 + step)
                return 0

            to(n_tp // 2)
            lax.fori_loop(1, n_tp // 2, pair, 0)
            part_recv[me_tp] = part_send[me_tp]
        with jax.named_scope("ring_wait"):
            at_row = lax.broadcasted_iota(jnp.int32, (8, batch), 0)
            at_col = lax.broadcasted_iota(jnp.int32, (8, batch), 1)
            pick = ((at_col == kept_rows * me_tp + at_row) & (at_row < kept_rows)).astype(BF16)
            h = jnp.concatenate([own_recv[j] for j in range(blocks)], axis=1)
            kept = jnp.dot(pick, h, preferred_element_type=F32)[0:kept_rows]
            window(l)
            total_wait(part_recv, n_tp - 1, recv_sem.at[ring_sum])
        with jax.named_scope("ring_sum"):
            tile = jnp.sum(part_recv[...].astype(F32), axis=0)
            update = jnp.concatenate(
                [tile[kept_rows * j : kept_rows * (j + 1)] for j in range(blocks)], axis=1
            )
            hidden_out[...] = (kept + update).astype(BF16)

    h_load.wait()
    project(0, h_v[...].astype(F32))
    with jax.named_scope("barrier"):
        pl.semaphore_wait(barrier, n_dp - 1 + 2 * blocks)
    for to in (blocks, -blocks):
        signal(know_sem.at[0], tp_at(to))
    with jax.named_scope("send_in0"):
        send_in(0)
        hist_load.wait()
        for l in range(layers):
            earlier(l)
        state_loads[0].wait()

    for l in range(layers):
        with jax.named_scope(f"in_wait{l}"):
            total_wait(in_recv.at[l], n_dp - 1, recv_sem.at[in_at(l)])
        mixer(l)
        if l == 0:
            pl.semaphore_wait(know_sem.at[0], 2)
            for to in (2 * blocks, -2 * blocks):
                signal(know_sem.at[1], tp_at(to))
        with jax.named_scope(f"mix_wait{l}"):
            send_mix(l)
            wo_loads[l].wait()
            if l == 0:
                window(l)
            total_wait(mix_recv.at[l], n_dp - 1, recv_sem.at[mix_at(l)])
        if l + 1 < layers:
            project(l + 1, reduce_all(l))
            with jax.named_scope(f"send_in{l + 1}"):
                send_in(l + 1)
                state_loads[l + 1].wait()
        else:
            reduce_rows(l)

    with jax.named_scope("end"):
        for l in range(layers):
            total_wait(in_send.at[l], n_dp - 1, send_sem.at[in_at(l)])
            total_wait(mix_recv.at[l], n_dp - 1, send_sem.at[mix_at(l)])
            pltpu.make_async_copy(state_v.at[l], state_out.at[l], state_sem).wait()
        total_wait(near_recv, blocks - 1, send_sem.at[near_sum])
        total_wait(far_recv, far - 1, send_sem.at[far_sum])
        total_wait(own_recv, blocks - 1, send_sem.at[near_all])
        total_wait(part_send, n_tp - 1, send_sem.at[ring_sum])


def body(n_tp, n_dp, *args):
    args = list(args)
    args[7] = jnp.transpose(args[7], (0, 2, 1))
    args[8] = jnp.transpose(args[8], (1, 2, 0, 3))
    args[9] = jnp.transpose(args[9], (0, 1, 3, 2, 4))
    args[13] = jnp.transpose(args[13], (0, 2, 1))
    h, w_value, history, state, w_out = (args[k] for k in (0, 3, 9, 14, 16))
    layers, feats, chans = w_value.shape
    batch = h.shape[0]
    rows = batch // n_dp
    roles, width_back = history.shape[2:4]
    blocks = feats // LANES
    vmem = pl.BlockSpec(memory_space=pltpu.VMEM)
    smem = pl.BlockSpec(memory_space=pltpu.SMEM)
    hbm = pl.BlockSpec(memory_space=pl.ANY)
    in_specs = [
        hbm, smem, vmem, hbm, hbm, hbm, hbm, vmem, vmem, hbm, smem, smem, smem, vmem, hbm, vmem, hbm,
    ]
    hidden, states, windows = pl.pallas_call(
        functools.partial(kernel, n_tp, n_dp),
        out_shape=(
            jax.ShapeDtypeStruct((batch // n_tp, feats), BF16),
            jax.ShapeDtypeStruct(state.shape, F32),
            jax.ShapeDtypeStruct(history.shape, BF16),
        ),
        in_specs=in_specs,
        out_specs=(vmem, hbm, vmem),
        scratch_shapes=[
            pltpu.VMEM((batch, feats), BF16),
            pltpu.VMEM((layers, feats, 4 * chans), BF16),
            pltpu.VMEM(w_out.shape, BF16),
            pltpu.VMEM(history.shape, BF16),
            pltpu.VMEM(state.shape, F32),
            pltpu.VMEM((rows * roles * width_back, LANES), F32),
            pltpu.VMEM((layers, rows * roles * width_back, LANES), F32),
            pltpu.VMEM((layers, roles, rows, LANES), F32),
            pltpu.VMEM((batch, LANES), F32),
            pltpu.VMEM((n_tp * 8, LANES), F32),
            pltpu.VMEM((layers, n_dp, 5, rows, LANES), BF16),
            pltpu.VMEM((layers, n_dp, 5, rows, LANES), BF16),
            pltpu.VMEM((layers, rows, LANES), BF16),
            pltpu.VMEM((layers, n_dp, rows, LANES), BF16),
            pltpu.VMEM((blocks, batch, LANES), BF16),
            pltpu.VMEM((blocks, batch, LANES), BF16),
            pltpu.VMEM((n_tp // blocks, batch, LANES), BF16),
            pltpu.VMEM((blocks, batch, LANES), BF16),
            pltpu.VMEM((n_tp, 8, LANES), BF16),
            pltpu.VMEM((n_tp, 8, LANES), BF16),
            pltpu.SemaphoreType.DMA((2 + 3 * layers,)),
            pltpu.SemaphoreType.DMA,
            pltpu.SemaphoreType.DMA((2 * layers + 4,)),
            pltpu.SemaphoreType.DMA((2 * layers + 4,)),
            pltpu.SemaphoreType.REGULAR((2,)),
        ],
        compiler_params=pltpu.CompilerParams(collective_id=0, has_side_effects=True),
    )(*args)
    return hidden, states, jnp.transpose(windows, (0, 1, 3, 2, 4))


def solution(mesh):
    placed = (
        P("grp", "dp"),
        P(("grp", "dp")),
        P(None, "dp"),
        P(None, "dp", "tp"),
        P(None, "dp", "tp"),
        P(None, "dp", "tp"),
        P(None, "dp", "tp"),
        P(None, "dp", None),
        P(None, None, None, "tp"),
        P(None, ("grp", "dp"), None, None, "tp"),
        P(None, "tp"),
        P(None, "tp"),
        P(None, "tp"),
        P(None, ("grp", "dp"), "tp"),
        P(None, ("grp", "dp"), "tp", None, None),
        P(None, "tp"),
        P(None, "tp", "dp"),
    )
    return jax.shard_map(
        functools.partial(body, mesh.shape["tp"], mesh.shape["dp"]),
        mesh=mesh,
        in_specs=placed,
        out_specs=(
            P(("grp", "tp"), "dp"),
            P(None, ("grp", "dp"), "tp", None, None),
            P(None, ("grp", "dp"), None, None, "tp"),
        ),
        check_vma=False,
    )
```

time: 115 us -> 109 us (0.948)
  local copies, waits for them, and re-layouts: 8.65 us -> 4.17 us
  Pallas kernels: 106 us -> 104 us
    unnamed x12 -> x7, local copies, waits for them, and re-layouts: 7.17 us -> 4.17 us
    pallas_call x1 -> x0, local copies, waits for them, and re-layouts: 1.48 us -> none  [body(): pl.pallas_call(functools.partial(kernel, n_tp, n_dp), out_shape=(jax.Shap...]
    pallas_call x1, Pallas kernels: 106 us -> 104 us  [body(): pl.pallas_call(functools.partial(kernel, n_tp, n_dp), out_shape=(jax.Shap...]
where the time goes in v2:
time: 109 us
  Pallas kernels  104 us (95%)
  local copies, waits for them, and re-layouts  4.17 us (4%)
    pallas_call x1, Pallas kernels, body(): pl.pallas_call(functools.partial(kernel, n_tp, n_dp), out_shape=(jax.Shap...  104 us
    unnamed x7, local copies, waits for them, and re-layouts  4.17 us

profile of v2, /device:TPU:40, one launch (start us, length us, event | category | flops | bytes accessed | tf_op | source)
XLA Modules:
  0.0 109.2 jit_solution(14418073654577869337)
XLA Ops:
  0.6 104.4 %shard_map.184 = (bf16[2,512]{1,0:T(2,128)(2,1)}, f32[2,8,2,64,128]{4,3,2,1,0:T(8,128)}, bf16[2,8,3,4,128]{4,3,2,1,0:T(4,128)(2,1)}) custom-call(bf16[64,512]{1,0:T(8,128)(2,1)} %h_in.1, s32[8]{0:T(128)} %counts.1, f32[2,512]{1,0:T(2,128)} %in_gain.1, bf16[2,512,128]{2,1,0:T(8,128)(2,1)} %w_value.1, bf16[2,512,128]{2,1,0:T(8,128)(2,1)} %w_inkey.1, ...), custom_call_target="tpu_custom_call" | custom-call | tf_op jit(solution)/shard_map/pallas_call | solution.py:415
  105.0 0.0 copy-start.1
  105.0 0.7 copy-done.1
  105.7 0.6 copy.23
  106.3 0.0 copy-start
  106.3 2.3 %copy.24 = f32[2,8,2,64,128]{4,3,2,1,0:T(8,128)} copy(f32[2,8,2,64,128]{4,3,2,1,0:T(8,128)} %get-tuple-element.13) | data formatting | bytes 2097152
  108.6 0.0 copy-done
  108.6 0.6 copy.25
Async XLA Ops:
  105.0 0.7 copy-start.1
  106.3 2.3 %copy-start = (bf16[2,8,3,4,128]{4,3,2,1,0:T(4,128)(2,1)S(1)}, bf16[2,8,3,4,128]{4,3,2,1,0:T(4,128)(2,1)}, u32[]{:S(2)}) copy-start(bf16[2,8,3,4,128]{4,3,2,1,0:T(4,128)(2,1)} %get-tuple-element.8) | copy-start | bytes 147460

commit v3 on v2

--- a/solution.py
+++ b/solution.py
@@ -25,25 +25,34 @@
     n_tp,
     n_dp,
     h_in,
-    counts,
-    in_gain,
+    counts_in,
+    in_gain_in,
     w_value,
     w_inkey,
     w_readkey,
     w_gate,
+    w_step_in,
+    taps_in,
+    history,
+    step_bias_in,
+    decay_log_in,
+    direct_gain_in,
+    extra_log_in,
+    state_in,
+    out_gain_in,
+    w_out,
+    hidden_out,
+    state_out,
+    window_out,
+    counts,
+    in_gain,
     w_step,
     taps,
-    history,
     step_bias,
     decay_log,
     direct_gain,
     extra_log,
-    state_in,
     out_gain,
-    w_out,
-    hidden_out,
-    state_out,
-    window_out,
     h_v,
     wp_v,
     wo_v,
@@ -52,20 +61,18 @@
     hist_f,
     win_f,
     early_v,
-    normed_f,
+    fixed_v,
     tile_f,
     in_send,
     in_recv,
-    mix_send,
     mix_recv,
-    near_send,
-    near_recv,
+    wide_recv,
+    wo_near,
     far_recv,
     own_recv,
     part_send,
     part_recv,
     load_sem,
-    state_sem,
     send_sem,
     recv_sem,
     know_sem,
@@ -107,21 +114,15 @@
 
     in_at = lambda l: l
     mix_at = lambda l: layers + l
-    near_sum, far_sum, near_all, ring_sum = (2 * layers + k for k in range(4))
-
-    barrier = pltpu.get_barrier_semaphore()
-    for shift in range(1, n_dp):
-        signal(barrier, dp_at(shift))
-    for shift in range(1, blocks + 1):
-        for to in (shift, -shift):
-            signal(barrier, tp_at(to))
+    weights_near, far_sum, near_all, ring_sum = (2 * layers + k for k in range(4))
+    dp_shifts = sorted(range(1, n_dp), key=lambda s: abs(s - n_dp // 2))
 
     def load(source, target, sem):
         copy = pltpu.make_async_copy(source, target, load_sem.at[sem])
         copy.start()
         return copy
 
-    h_load = load(h_in, h_v, 0)
+    h_load = [load(h_in, h_v, 0), load(in_gain_in, in_gain, 0)]
     w_loads, state_loads, wo_loads = [], [], []
     for l in range(layers):
         w_loads.append(
@@ -131,9 +132,29 @@
             ]
         )
         if l == 0:
-            hist_load = load(history, hist_v, 1 + layers)
-        state_loads.append(load(state_in.at[l], state_v.at[l], 2 + layers + l))
-        wo_loads.append(load(w_out.at[l], wo_v.at[l], 2 + 2 * layers + l))
+            step_load = load(w_step_in, w_step, 1 + layers)
+            small_loads = [
+                load(source, target, 2 + layers)
+                for source, target in (
+                    (history, hist_v),
+                    (counts_in, counts),
+                    (taps_in, taps),
+                    (step_bias_in, step_bias),
+                    (decay_log_in, decay_log),
+                    (direct_gain_in, direct_gain),
+                    (extra_log_in, extra_log),
+                    (out_gain_in, out_gain),
+                )
+            ]
+        state_loads.append(load(state_in.at[l], state_v.at[l], 3 + layers + l))
+        wo_loads.append(load(w_out.at[l], wo_v.at[l], 3 + 2 * layers + l))
+
+    barrier = pltpu.get_barrier_semaphore()
+    for shift in range(1, n_dp):
+        signal(barrier, dp_at(shift))
+    for shift in range(1, blocks + 1):
+        for to in (shift, -shift):
+            signal(barrier, tp_at(to))
 
     lane = lax.broadcasted_iota(jnp.int32, (rows, LANES), 1)
     lane_all = lax.broadcasted_iota(jnp.int32, (batch, LANES), 1)
@@ -147,6 +168,8 @@
         with jax.named_scope(f"proj{l}"):
             squares = jnp.sum(h * h, axis=1, keepdims=True)
             scaled = (h * in_gain[l : l + 1, :]).astype(BF16)
+            if l == 0:
+                step_load.wait()
             steps = lax.dot_general(
                 scaled, w_step[l], (((1,), (1,)), ((), ())), preferred_element_type=F32
             )
@@ -157,8 +180,9 @@
                 )
                 for k in range(heads)
             ] + [squares]
-            for load in w_loads[l]:
-                load.wait()
+            if l == 0:
+                for copy in w_loads[l]:
+                    copy.wait()
             part = jnp.dot(scaled, wp_v[l], preferred_element_type=F32)
             stats = jnp.zeros((batch, LANES), F32)
             for k, v in enumerate(wanted):
@@ -172,7 +196,7 @@
                 in_send[l, i, 4] = stats[at].astype(BF16)
 
     def send_in(l):
-        for shift in range(1, n_dp):
+        for shift in dp_shifts:
             to = dp_at(shift)
             remote(in_send.at[l, to["dp"]], in_recv.at[l, me_dp], in_at(l), to)
         in_recv[l, me_dp] = in_send[l, me_dp]
@@ -197,6 +221,17 @@
                         l, pl.ds(r * width_back + j - 1, rows, stride=roles * width_back), :
                     ] = past
             early_v[l, r] = total
+        diagonal = lax.broadcasted_iota(jnp.int32, (rows, rows), 0) == lax.broadcasted_iota(
+            jnp.int32, (rows, rows), 1
+        )
+        extra = [
+            jnp.sum(jnp.where(diagonal, extra_log[l, k : k + 1, :], 0.0), axis=1, keepdims=True)
+            for k in range(heads)
+        ]
+        fixed_v[l, 0] = jnp.where(first_head, extra[0], extra[1])
+        fixed_v[l, 1] = jnp.exp(spread(decay_log, l))
+        fixed_v[l, 2] = spread(step_bias, l)
+        fixed_v[l, 3] = spread(direct_gain, l)
 
     def window(l):
         for b in range(rows):
@@ -225,18 +260,8 @@
                 )
                 for r in range(roles)
             ]
-            rate = jax.nn.softplus(step + spread(step_bias, l))
-            diagonal = lax.broadcasted_iota(
-                jnp.int32, (rows, rows), 0
-            ) == lax.broadcasted_iota(jnp.int32, (rows, rows), 1)
-            extra = [
-                jnp.sum(
-                    jnp.where(diagonal, extra_log[l, k : k + 1, :], 0.0), axis=1, keepdims=True
-                )
-                for k in range(heads)
-            ]
-            extra = jnp.where(first_head, extra[0], extra[1])
-            decay = jnp.exp(-rate * jnp.exp(spread(decay_log, l)) + extra)
+            rate = jax.nn.softplus(step + fixed_v[l, 2])
+            decay = jnp.exp(-rate * fixed_v[l, 1] + fixed_v[l, 0])
             gain = rate * value
             gain_t = jnp.transpose(jnp.concatenate([gain] * (LANES // rows), axis=0))
             lane_sq = lax.broadcasted_iota(jnp.int32, (head_dim, LANES), 1)
@@ -248,52 +273,72 @@
                     decay_b = decay[b : b + 1, k * head_dim : k * head_dim + 1]
                     column = gain_t[k * head_dim : (k + 1) * head_dim, b : b + 1]
                     new = decay_b * state_v[l, b, k] + column * key_b
-                    state_v[l, b, k] = new
+                    state_out[l, b, k] = new
                     read = jnp.sum(new * read_b, axis=1, keepdims=True)
                     reads[k] = jnp.where(lane_sq == b, read, reads[k])
             readout = jnp.transpose(jnp.concatenate(reads, axis=0))[0:rows]
-            readout = readout + spread(direct_gain, l) * value
+            readout = readout + fixed_v[l, 3] * value
             gated = readout * jax.nn.silu(gate)
             scale = lax.rsqrt(jnp.mean(gated * gated, axis=1, keepdims=True) + EPSILON)
             normed = (gated * scale * out_gain[l : l + 1, :]).astype(BF16)
-            mix_send[l] = normed
-            mix_recv[l, me_dp] = normed
+            if l + 1 < layers:
+                wide_recv[me_quarter * n_dp + me_dp] = normed
+            else:
+                mix_recv[me_dp] = normed
             for r in range(roles):
                 win_f[
                     l, pl.ds((r + 1) * width_back - 1, rows, stride=roles * width_back), :
                 ] = current[r]
 
     def send_mix(l):
-        for shift in range(1, n_dp):
-            remote(mix_send.at[l], mix_recv.at[l, me_dp], mix_at(l), dp_at(shift))
-        pltpu.make_async_copy(state_v.at[l], state_out.at[l], state_sem).start()
-
-    def reduce_all(l):
-        with jax.named_scope("near_sum"):
+        if l + 1 < layers:
+            here = wide_recv.at[me_quarter * n_dp + me_dp]
+            for shift in dp_shifts:
+                for near in range(1, blocks):
+                    remote(here, here, mix_at(l), near_at(near) | dp_at(shift))
+            for near in range(1, blocks):
+                remote(here, here, mix_at(l), near_at(near))
+        else:
+            here = mix_recv.at[me_dp]
+        for shift in dp_shifts:
+            remote(here, here, mix_at(l), dp_at(shift))
+
+    def wait_mix(l, sem):
+        if l + 1 < layers:
+            total_wait(wide_recv, blocks * n_dp - 1, sem)
+        else:
+            total_wait(mix_recv, n_dp - 1, sem)
+
+    def send_weights():
+        for near in range(1, blocks):
+            quarter = lax.rem(me_quarter + near, blocks)
+            columns = pl.ds(pl.multiple_of(quarter * LANES, LANES), LANES)
+            remote(wo_v.at[0, :, columns], wo_near.at[me_quarter], weights_near, near_at(near))
+        columns = pl.ds(pl.multiple_of(me_quarter * LANES, LANES), LANES)
+        wo_near[me_quarter] = wo_v[0, :, columns]
+
+    def reduce_all():
+        with jax.named_scope("far_send"):
             mix = jnp.concatenate(
-                [mix_recv[l, i].astype(F32) for i in range(n_dp)], axis=0
-            ).astype(BF16)
-            part = jnp.dot(mix, wo_v[l], preferred_element_type=F32)
-            for j in range(blocks):
-                near_send[j] = part[:, j * LANES : (j + 1) * LANES].astype(BF16)
-            for shift in range(1, blocks):
-                to = near_at(shift)
-                quarter = lax.rem(me_quarter + shift, blocks)
-                remote(near_send.at[quarter], near_recv.at[me_quarter], near_sum, to)
-            near_recv[me_quarter] = near_send[me_quarter]
-            h = h_v[:, pl.ds(pl.multiple_of(me_quarter * LANES, LANES), LANES)].astype(F32)
-        with jax.named_scope("near_wait"):
-            total_wait(near_recv, blocks - 1, recv_sem.at[near_sum])
-        with jax.named_scope("far_send"):
-            far_recv[me_block] = jnp.sum(near_recv[...].astype(F32), axis=0).astype(BF16)
+                [
+                    jnp.concatenate(
+                        [wide_recv[q * n_dp + i].astype(F32) for i in range(n_dp)], axis=0
+                    ).astype(BF16)
+                    for q in range(blocks)
+                ],
+                axis=1,
+            )
+            part = jnp.dot(
+                mix, wo_near[...].reshape(-1, LANES), preferred_element_type=F32
+            )
+            far_recv[me_block] = part.astype(BF16)
             pl.semaphore_wait(know_sem.at[1], 2)
             for step in range(far // 2, 0, -1):
                 for shift in sorted({step, far - step}):
                     to = tp_at(shift * blocks)
                     remote(far_recv.at[me_block], far_recv.at[me_block], far_sum, to)
+            h = h_v[:, pl.ds(pl.multiple_of(me_quarter * LANES, LANES), LANES)].astype(F32)
         with jax.named_scope("far_wait"):
-            for load in w_loads[l + 1]:
-                pass
             total_wait(far_recv, far - 1, recv_sem.at[far_sum])
         with jax.named_scope("near_all"):
             mine = (h + jnp.sum(far_recv[...].astype(F32), axis=0)).astype(BF16)
@@ -306,18 +351,13 @@
 
     def reduce_rows(l):
         with jax.named_scope("ring_send"):
-            for i in range(n_dp):
-                normed_f[i * rows : (i + 1) * rows, :] = mix_recv[l, i].astype(F32)
             kept_rows = batch // n_tp
             mix = jnp.concatenate(
-                [normed_f[pl.ds(r, n_tp, stride=kept_rows), :] for r in range(kept_rows)], axis=0
+                [mix_recv[i].astype(F32) for i in range(n_dp)], axis=0
             ).astype(BF16)
             part = jnp.dot(mix, wo_v[l], preferred_element_type=F32)
             for j in range(blocks):
-                for r in range(kept_rows):
-                    tile_f[pl.ds(kept_rows * j + r, n_tp, stride=8), :] = part[
-                        r * n_tp : (r + 1) * n_tp, j * LANES : (j + 1) * LANES
-                    ]
+                tile_f[pl.ds(j, batch, stride=blocks), :] = part[:, j * LANES : (j + 1) * LANES]
             for i in range(n_tp):
                 part_send[i] = tile_f[i * 8 : (i + 1) * 8, :].astype(BF16)
 
@@ -342,21 +382,26 @@
             window(l)
             total_wait(part_recv, n_tp - 1, recv_sem.at[ring_sum])
         with jax.named_scope("ring_sum"):
-            tile = jnp.sum(part_recv[...].astype(F32), axis=0)
+            tile_f[0:8, :] = jnp.sum(part_recv[...].astype(F32), axis=0)
             update = jnp.concatenate(
-                [tile[kept_rows * j : kept_rows * (j + 1)] for j in range(blocks)], axis=1
+                [tile_f[pl.ds(j, kept_rows, stride=blocks), :] for j in range(blocks)], axis=1
             )
             hidden_out[...] = (kept + update).astype(BF16)
 
-    h_load.wait()
+    with jax.named_scope("load_wait"):
+        for copy in h_load:
+            copy.wait()
     project(0, h_v[...].astype(F32))
     with jax.named_scope("barrier"):
         pl.semaphore_wait(barrier, n_dp - 1 + 2 * blocks)
-    for to in (blocks, -blocks):
-        signal(know_sem.at[0], tp_at(to))
     with jax.named_scope("send_in0"):
         send_in(0)
-        hist_load.wait()
+        for to in (blocks, -blocks):
+            signal(know_sem.at[0], tp_at(to))
+        wo_loads[0].wait()
+        send_weights()
+        for copy in small_loads:
+            copy.wait()
         for l in range(layers):
             earlier(l)
         state_loads[0].wait()
@@ -365,33 +410,54 @@
         with jax.named_scope(f"in_wait{l}"):
             total_wait(in_recv.at[l], n_dp - 1, recv_sem.at[in_at(l)])
         mixer(l)
-        if l == 0:
-            pl.semaphore_wait(know_sem.at[0], 2)
-            for to in (2 * blocks, -2 * blocks):
-                signal(know_sem.at[1], tp_at(to))
+        with jax.named_scope(f"send_mix{l}"):
+            send_mix(l)
+            if l == 0:
+                pl.semaphore_wait(know_sem.at[0], 2)
+                for to in (2 * blocks, -2 * blocks):
+                    signal(know_sem.at[1], tp_at(to))
+                window(l)
+                total_wait(wo_near, blocks - 1, recv_sem.at[weights_near])
+                for copy in w_loads[1]:
+                    copy.wait()
         with jax.named_scope(f"mix_wait{l}"):
-            send_mix(l)
-            wo_loads[l].wait()
-            if l == 0:
-                window(l)
-            total_wait(mix_recv.at[l], n_dp - 1, recv_sem.at[mix_at(l)])
+            wait_mix(l, recv_sem.at[mix_at(l)])
         if l + 1 < layers:
-            project(l + 1, reduce_all(l))
+            project(l + 1, reduce_all())
             with jax.named_scope(f"send_in{l + 1}"):
                 send_in(l + 1)
                 state_loads[l + 1].wait()
+                wo_loads[l + 1].wait()
         else:
             reduce_rows(l)
 
     with jax.named_scope("end"):
         for l in range(layers):
             total_wait(in_send.at[l], n_dp - 1, send_sem.at[in_at(l)])
-            total_wait(mix_recv.at[l], n_dp - 1, send_sem.at[mix_at(l)])
-            pltpu.make_async_copy(state_v.at[l], state_out.at[l], state_sem).wait()
-        total_wait(near_recv, blocks - 1, send_sem.at[near_sum])
+            wait_mix(l, send_sem.at[mix_at(l)])
+        total_wait(wo_near, blocks - 1, send_sem.at[weights_near])
         total_wait(far_recv, far - 1, send_sem.at[far_sum])
         total_wait(own_recv, blocks - 1, send_sem.at[near_all])
         total_wait(part_send, n_tp - 1, send_sem.at[ring_sum])
+
+
+def write_out(pieces, hidden_v, states_v, windows_v, hidden, states, windows, sem):
+    copies = [
+        pltpu.make_async_copy(hidden_v, hidden, sem.at[0]),
+        pltpu.make_async_copy(windows_v, windows, sem.at[1]),
+    ]
+    layers, batch = states.shape[:2]
+    step = layers * batch // pieces
+    for p in range(pieces):
+        l, b = divmod(p * step, batch)
+        part = pl.ds(b, step)
+        copies.append(
+            pltpu.make_async_copy(states_v.at[l, part], states.at[l, part], sem.at[2 + p])
+        )
+    for copy in copies:
+        copy.start()
+    for copy in copies:
+        copy.wait()
 
 
 def body(n_tp, n_dp, *args):
@@ -407,21 +473,20 @@
     roles, width_back = history.shape[2:4]
     blocks = feats // LANES
     vmem = pl.BlockSpec(memory_space=pltpu.VMEM)
-    smem = pl.BlockSpec(memory_space=pltpu.SMEM)
     hbm = pl.BlockSpec(memory_space=pl.ANY)
-    in_specs = [
-        hbm, smem, vmem, hbm, hbm, hbm, hbm, vmem, vmem, hbm, smem, smem, smem, vmem, hbm, vmem, hbm,
-    ]
-    hidden, states, windows = pl.pallas_call(
+    kept = pltpu.VMEM((batch // n_tp, feats), BF16), pltpu.VMEM(state.shape, F32), pltpu.VMEM(
+        history.shape, BF16
+    )
+    in_vmem = pl.pallas_call(
         functools.partial(kernel, n_tp, n_dp),
-        out_shape=(
-            jax.ShapeDtypeStruct((batch // n_tp, feats), BF16),
-            jax.ShapeDtypeStruct(state.shape, F32),
-            jax.ShapeDtypeStruct(history.shape, BF16),
-        ),
-        in_specs=in_specs,
-        out_specs=(vmem, hbm, vmem),
+        out_shape=kept,
+        in_specs=[hbm] * len(args),
+        out_specs=(vmem, vmem, vmem),
         scratch_shapes=[
+            pltpu.SMEM(args[1].shape, args[1].dtype),
+            *(pltpu.VMEM(args[k].shape, args[k].dtype) for k in (2, 7, 8)),
+            *(pltpu.SMEM(args[k].shape, args[k].dtype) for k in (10, 11, 12)),
+            *(pltpu.VMEM(args[k].shape, args[k].dtype) for k in (13, 15)),
             pltpu.VMEM((batch, feats), BF16),
             pltpu.VMEM((layers, feats, 4 * chans), BF16),
             pltpu.VMEM(w_out.shape, BF16),
@@ -430,26 +495,32 @@
             pltpu.VMEM((rows * roles * width_back, LANES), F32),
             pltpu.VMEM((layers, rows * roles * width_back, LANES), F32),
             pltpu.VMEM((layers, roles, rows, LANES), F32),
-            pltpu.VMEM((batch, LANES), F32),
+            pltpu.VMEM((layers, 4, rows, LANES), F32),
             pltpu.VMEM((n_tp * 8, LANES), F32),
             pltpu.VMEM((layers, n_dp, 5, rows, LANES), BF16),
             pltpu.VMEM((layers, n_dp, 5, rows, LANES), BF16),
-            pltpu.VMEM((layers, rows, LANES), BF16),
-            pltpu.VMEM((layers, n_dp, rows, LANES), BF16),
-            pltpu.VMEM((blocks, batch, LANES), BF16),
-            pltpu.VMEM((blocks, batch, LANES), BF16),
+            pltpu.VMEM((n_dp, rows, LANES), BF16),
+            pltpu.VMEM((blocks * n_dp, rows, LANES), BF16),
+            pltpu.VMEM((blocks, chans, LANES), BF16),
             pltpu.VMEM((n_tp // blocks, batch, LANES), BF16),
             pltpu.VMEM((blocks, batch, LANES), BF16),
             pltpu.VMEM((n_tp, 8, LANES), BF16),
             pltpu.VMEM((n_tp, 8, LANES), BF16),
-            pltpu.SemaphoreType.DMA((2 + 3 * layers,)),
-            pltpu.SemaphoreType.DMA,
+            pltpu.SemaphoreType.DMA((3 + 3 * layers,)),
             pltpu.SemaphoreType.DMA((2 * layers + 4,)),
             pltpu.SemaphoreType.DMA((2 * layers + 4,)),
             pltpu.SemaphoreType.REGULAR((2,)),
         ],
         compiler_params=pltpu.CompilerParams(collective_id=0, has_side_effects=True),
     )(*args)
+    pieces = 4
+    hidden, states, windows = pl.pallas_call(
+        functools.partial(write_out, pieces),
+        out_shape=tuple(jax.ShapeDtypeStruct(k.shape, k.dtype) for k in in_vmem),
+        in_specs=[vmem] * 3,
+        out_specs=(hbm, hbm, hbm),
+        scratch_shapes=[pltpu.SemaphoreType.DMA((2 + pieces,))],
+    )(*(pltpu.with_memory_space_constraint(k, pltpu.VMEM) for k in in_vmem))
     return hidden, states, jnp.transpose(windows, (0, 1, 3, 2, 4))
 
 

time: 109 us -> 103 us (0.945)
  local copies, waits for them, and re-layouts: 4.17 us -> 0 us
  Pallas kernels: 104 us -> 102 us
    unnamed x7 -> x0, local copies, waits for them, and re-layouts: 4.17 us -> none
    pallas_call x1 -> x2, Pallas kernels: 104 us -> 102 us  [the longest x1 101 us: body(): pl.pallas_call(functools.partial(kernel, n_tp, n_dp), out_shape=kept, in_...]
where the time goes in v3:
time: 103 us
  Pallas kernels  102 us (99%)
    pallas_call x1, Pallas kernels, body(): pl.pallas_call(functools.partial(kernel, n_tp, n_dp), out_shape=kept, in_...  101 us

profile of v3, /device:TPU:40, one launch (start us, length us, event | category | flops | bytes accessed | tf_op | source)
XLA Modules:
  0.0 103.1 jit_solution(10703603924472469564)
XLA Ops:
  0.6 101.4 %shard_map.184 = (bf16[2,512]{1,0:T(2,128)(2,1)S(1)}, f32[2,8,2,64,128]{4,3,2,1,0:T(8,128)S(1)}, bf16[2,8,3,4,128]{4,3,2,1,0:T(4,128)(2,1)S(1)}) custom-call(bf16[64,512]{1,0:T(8,128)(2,1)} %h_in.1, s32[8]{0:T(128)} %counts_in.1, f32[2,512]{1,0:T(2,128)} %in_gain_in.1, bf16[2,512,128]{2,1,0:T(8,128)(2,1)} %w_value.1, bf16[2,512,128]{2,1,0:T(8,128)(2,1)} %w_inkey.1, ...), custom_call_target="tpu_custom_call" | custom-call | tf_op jit(solution)/shard_map/pallas_call | solution.py:480
  102.1 1.0 %shard_map.185 = (bf16[2,512]{1,0:T(2,128)(2,1)}, f32[2,8,2,64,128]{4,3,2,1,0:T(8,128)}, bf16[2,8,3,4,128]{4,3,2,1,0:T(4,128)(2,1)}) custom-call(bf16[2,512]{1,0:T(2,128)(2,1)S(1)} %get-tuple-element.9.hidden_v, f32[2,8,2,64,128]{4,3,2,1,0:T(8,128)S(1)} %get-tuple-element.10.states_v, bf16[2,8,3,4,128]{4,3,2,1,0:T(4,128)(2,1)S(1)} %get-tuple-element.11.windows_v), custom_call_target="tpu_custom_call" | custom-call | tf_op jit(solution)/shard_map/pallas_call | solution.py:517

commit v4 on v3

--- a/solution.py
+++ b/solution.py
@@ -122,32 +122,15 @@
         copy.start()
         return copy
 
+    def load_products(l):
+        return [
+            load(w.at[l], wp_v.at[l, :, pl.ds(k * LANES, LANES)], 1 + l)
+            for k, w in enumerate((w_value, w_inkey, w_readkey, w_gate))
+        ]
+
     h_load = [load(h_in, h_v, 0), load(in_gain_in, in_gain, 0)]
-    w_loads, state_loads, wo_loads = [], [], []
-    for l in range(layers):
-        w_loads.append(
-            [
-                load(w.at[l], wp_v.at[l, :, pl.ds(k * LANES, LANES)], 1 + l)
-                for k, w in enumerate((w_value, w_inkey, w_readkey, w_gate))
-            ]
-        )
-        if l == 0:
-            step_load = load(w_step_in, w_step, 1 + layers)
-            small_loads = [
-                load(source, target, 2 + layers)
-                for source, target in (
-                    (history, hist_v),
-                    (counts_in, counts),
-                    (taps_in, taps),
-                    (step_bias_in, step_bias),
-                    (decay_log_in, decay_log),
-                    (direct_gain_in, direct_gain),
-                    (extra_log_in, extra_log),
-                    (out_gain_in, out_gain),
-                )
-            ]
-        state_loads.append(load(state_in.at[l], state_v.at[l], 3 + layers + l))
-        wo_loads.append(load(w_out.at[l], wo_v.at[l], 3 + 2 * layers + l))
+    w_loads = [load_products(0)]
+    step_load = load(w_step_in, w_step, 1 + layers)
 
     barrier = pltpu.get_barrier_semaphore()
     for shift in range(1, n_dp):
@@ -160,6 +143,14 @@
     lane_all = lax.broadcasted_iota(jnp.int32, (batch, LANES), 1)
     sub = lax.broadcasted_iota(jnp.int32, (rows, LANES), 0)
     first_head = lane < head_dim
+    unit = (
+        lax.broadcasted_iota(jnp.int32, (LANES, LANES), 0)
+        == lax.broadcasted_iota(jnp.int32, (LANES, LANES), 1)
+    ).astype(BF16)
+
+    def halves(x):
+        high = x.astype(BF16)
+        return high, (x - high.astype(F32)).astype(BF16)
 
     def spread(values, in_layer):
         return jnp.where(first_head, values[in_layer, 0], values[in_layer, 1])
@@ -263,20 +254,40 @@
             rate = jax.nn.softplus(step + fixed_v[l, 2])
             decay = jnp.exp(-rate * fixed_v[l, 1] + fixed_v[l, 0])
             gain = rate * value
-            gain_t = jnp.transpose(jnp.concatenate([gain] * (LANES // rows), axis=0))
-            lane_sq = lax.broadcasted_iota(jnp.int32, (head_dim, LANES), 1)
-            reads = [jnp.zeros((head_dim, LANES), F32) for _ in range(heads)]
+            high, low = halves(gain)
+            none = jnp.zeros((LANES - 3 * rows, LANES), BF16)
+            parts = jnp.concatenate([high, high, low, none], axis=0)
+            columns = lax.dot_general(
+                unit, parts, (((1,), (1,)), ((), ())), preferred_element_type=F32
+            )
+            lane_sq = lax.broadcasted_iota(jnp.int32, (LANES, LANES), 1)
+            left = jnp.concatenate(
+                [jnp.where(lane_sq % rows == b, columns, 0.0).astype(BF16) for b in range(rows)],
+                axis=0,
+            )
+            high, low = halves(inkey)
+            right = jnp.concatenate([high, low, high, none], axis=0)
+            outer = jnp.dot(left, right, preferred_element_type=F32)
+            reader = readkey.astype(BF16)
+            fades = [
+                jnp.broadcast_to(decay[:, k * head_dim : k * head_dim + 1], (rows, LANES))
+                for k in range(heads)
+            ]
+            readout = jnp.zeros((rows, LANES), F32)
             for b in range(rows):
-                key_b = jnp.broadcast_to(inkey[b : b + 1], (head_dim, LANES))
-                read_b = jnp.broadcast_to(readkey[b : b + 1], (head_dim, LANES))
+                news = []
                 for k in range(heads):
-                    decay_b = decay[b : b + 1, k * head_dim : k * head_dim + 1]
-                    column = gain_t[k * head_dim : (k + 1) * head_dim, b : b + 1]
-                    new = decay_b * state_v[l, b, k] + column * key_b
+                    at = (b * heads + k) * head_dim
+                    new = fades[k][b : b + 1] * state_v[l, b, k] + outer[at : at + head_dim]
                     state_out[l, b, k] = new
-                    read = jnp.sum(new * read_b, axis=1, keepdims=True)
-                    reads[k] = jnp.where(lane_sq == b, read, reads[k])
-            readout = jnp.transpose(jnp.concatenate(reads, axis=0))[0:rows]
+                    news.append(new.astype(BF16))
+                read = lax.dot_general(
+                    reader,
+                    jnp.concatenate(news, axis=0),
+                    (((1,), (1,)), ((), ())),
+                    preferred_element_type=F32,
+                )
+                readout = jnp.where(sub == b, read, readout)
             readout = readout + fixed_v[l, 3] * value
             gated = readout * jax.nn.silu(gate)
             scale = lax.rsqrt(jnp.mean(gated * gated, axis=1, keepdims=True) + EPSILON)
@@ -398,24 +409,45 @@
         send_in(0)
         for to in (blocks, -blocks):
             signal(know_sem.at[0], tp_at(to))
-        wo_loads[0].wait()
-        send_weights()
+        small_loads = [
+            load(source, target, 2 + layers)
+            for source, target in (
+                (history, hist_v),
+                (counts_in, counts),
+                (taps_in, taps),
+                (step_bias_in, step_bias),
+                (decay_log_in, decay_log),
+                (direct_gain_in, direct_gain),
+                (extra_log_in, extra_log),
+                (out_gain_in, out_gain),
+            )
+        ]
+        state_loads = [load(state_in.at[0], state_v.at[0], 3 + layers)]
+        wo_loads = [load(w_out.at[0], wo_v.at[0], 3 + 2 * layers)]
+        for l in range(1, layers):
+            w_loads.append(load_products(l))
+            state_loads.append(load(state_in.at[l], state_v.at[l], 3 + layers + l))
+            wo_loads.append(load(w_out.at[l], wo_v.at[l], 3 + 2 * layers + l))
         for copy in small_loads:
             copy.wait()
         for l in range(layers):
             earlier(l)
+        wo_loads[0].wait()
+        send_weights()
         state_loads[0].wait()
 
     for l in range(layers):
         with jax.named_scope(f"in_wait{l}"):
             total_wait(in_recv.at[l], n_dp - 1, recv_sem.at[in_at(l)])
+        if l == 0:
+            with jax.named_scope("know"):
+                pl.semaphore_wait(know_sem.at[0], 2)
+                for to in (2 * blocks, -2 * blocks):
+                    signal(know_sem.at[1], tp_at(to))
         mixer(l)
         with jax.named_scope(f"send_mix{l}"):
             send_mix(l)
             if l == 0:
-                pl.semaphore_wait(know_sem.at[0], 2)
-                for to in (2 * blocks, -2 * blocks):
-                    signal(know_sem.at[1], tp_at(to))
                 window(l)
                 total_wait(wo_near, blocks - 1, recv_sem.at[weights_near])
                 for copy in w_loads[1]:

time: 103 us -> 102 us (level)
    pallas_call x1, Pallas kernels: 101 us -> 100 us  [body(): pl.pallas_call(functools.partial(kernel, n_tp, n_dp), out_shape=kept, in_...]
where the time goes in v4:
time: 102 us
  Pallas kernels  101 us (99%)
    pallas_call x1, Pallas kernels, body(): pl.pallas_call(functools.partial(kernel, n_tp, n_dp), out_shape=kept, in_...  100 us

profile of v4, /device:TPU:40, one launch (start us, length us, event | category | flops | bytes accessed | tf_op | source)
XLA Modules:
  0.0 101.9 jit_solution(5107372075089947144)
XLA Ops:
  0.6 100.3 %shard_map.184 = (bf16[2,512]{1,0:T(2,128)(2,1)S(1)}, f32[2,8,2,64,128]{4,3,2,1,0:T(8,128)S(1)}, bf16[2,8,3,4,128]{4,3,2,1,0:T(4,128)(2,1)S(1)}) custom-call(bf16[64,512]{1,0:T(8,128)(2,1)} %h_in.1, s32[8]{0:T(128)} %counts_in.1, f32[2,512]{1,0:T(2,128)} %in_gain_in.1, bf16[2,512,128]{2,1,0:T(8,128)(2,1)} %w_value.1, bf16[2,512,128]{2,1,0:T(8,128)(2,1)} %w_inkey.1, ...), custom_call_target="tpu_custom_call" | custom-call | tf_op jit(solution)/shard_map/pallas_call | solution.py:512
  100.9 1.0 %shard_map.185 = (bf16[2,512]{1,0:T(2,128)(2,1)}, f32[2,8,2,64,128]{4,3,2,1,0:T(8,128)}, bf16[2,8,3,4,128]{4,3,2,1,0:T(4,128)(2,1)}) custom-call(bf16[2,512]{1,0:T(2,128)(2,1)S(1)} %get-tuple-element.9.hidden_v, f32[2,8,2,64,128]{4,3,2,1,0:T(8,128)S(1)} %get-tuple-element.10.states_v, bf16[2,8,3,4,128]{4,3,2,1,0:T(4,128)(2,1)S(1)} %get-tuple-element.11.windows_v), custom_call_target="tpu_custom_call" | custom-call | tf_op jit(solution)/shard_map/pallas_call | solution.py:549

commit v5 on v4

--- a/solution.py
+++ b/solution.py
@@ -68,6 +68,7 @@
     mix_recv,
     wide_recv,
     wo_near,
+    pair_v,
     far_recv,
     own_recv,
     part_send,
@@ -84,11 +85,13 @@
     head_dim = state_in.shape[3]
     heads = state_in.shape[2]
     roles, width_back = history.shape[2:4]
-    far = n_tp // blocks
+    far = n_tp // (2 * blocks)
     me_tp = lax.axis_index("tp")
     me_dp = lax.axis_index("dp")
     me_block = me_tp // blocks
     me_quarter = lax.rem(me_tp, blocks)
+    me_pair = me_block // 2
+    odd = lax.rem(me_block, 2)
 
     def tp_at(shift):
         return {"tp": lax.rem(me_tp + (n_tp + shift), n_tp)}
@@ -114,7 +117,7 @@
 
     in_at = lambda l: l
     mix_at = lambda l: layers + l
-    weights_near, far_sum, near_all, ring_sum = (2 * layers + k for k in range(4))
+    weights_near, far_sum, near_all, ring_sum, pair_sum = (2 * layers + k for k in range(5))
     dp_shifts = sorted(range(1, n_dp), key=lambda s: abs(s - n_dp // 2))
 
     def load(source, target, sem):
@@ -342,13 +345,18 @@
             part = jnp.dot(
                 mix, wo_near[...].reshape(-1, LANES), preferred_element_type=F32
             )
-            far_recv[me_block] = part.astype(BF16)
+            pair_v[0] = part.astype(BF16)
+            remote(pair_v.at[0], pair_v.at[1], pair_sum, {"tp": me_tp + blocks - 2 * blocks * odd})
+            h = h_v[:, pl.ds(pl.multiple_of(me_quarter * LANES, LANES), LANES)].astype(F32)
+        with jax.named_scope("pair_wait"):
+            total_wait(pair_v, 1, recv_sem.at[pair_sum])
+        with jax.named_scope("pair_send"):
+            far_recv[me_pair] = (pair_v[0].astype(F32) + pair_v[1].astype(F32)).astype(BF16)
             pl.semaphore_wait(know_sem.at[1], 2)
             for step in range(far // 2, 0, -1):
                 for shift in sorted({step, far - step}):
-                    to = tp_at(shift * blocks)
-                    remote(far_recv.at[me_block], far_recv.at[me_block], far_sum, to)
-            h = h_v[:, pl.ds(pl.multiple_of(me_quarter * LANES, LANES), LANES)].astype(F32)
+                    to = tp_at(shift * 2 * blocks)
+                    remote(far_recv.at[me_pair], far_recv.at[me_pair], far_sum, to)
         with jax.named_scope("far_wait"):
             total_wait(far_recv, far - 1, recv_sem.at[far_sum])
         with jax.named_scope("near_all"):
@@ -439,15 +447,13 @@
     for l in range(layers):
         with jax.named_scope(f"in_wait{l}"):
             total_wait(in_recv.at[l], n_dp - 1, recv_sem.at[in_at(l)])
-        if l == 0:
-            with jax.named_scope("know"):
-                pl.semaphore_wait(know_sem.at[0], 2)
-                for to in (2 * blocks, -2 * blocks):
-                    signal(know_sem.at[1], tp_at(to))
         mixer(l)
         with jax.named_scope(f"send_mix{l}"):
             send_mix(l)
             if l == 0:
+                pl.semaphore_wait(know_sem.at[0], 2)
+                for to in (2 * blocks, -2 * blocks):
+                    signal(know_sem.at[1], tp_at(to))
                 window(l)
                 total_wait(wo_near, blocks - 1, recv_sem.at[weights_near])
                 for copy in w_loads[1]:
@@ -469,6 +475,7 @@
             wait_mix(l, send_sem.at[mix_at(l)])
         total_wait(wo_near, blocks - 1, send_sem.at[weights_near])
         total_wait(far_recv, far - 1, send_sem.at[far_sum])
+        total_wait(pair_v, 1, send_sem.at[pair_sum])
         total_wait(own_recv, blocks - 1, send_sem.at[near_all])
         total_wait(part_send, n_tp - 1, send_sem.at[ring_sum])
 
@@ -534,13 +541,14 @@
             pltpu.VMEM((n_dp, rows, LANES), BF16),
             pltpu.VMEM((blocks * n_dp, rows, LANES), BF16),
             pltpu.VMEM((blocks, chans, LANES), BF16),
-            pltpu.VMEM((n_tp // blocks, batch, LANES), BF16),
+            pltpu.VMEM((2, batch, LANES), BF16),
+            pltpu.VMEM((n_tp // (2 * blocks), batch, LANES), BF16),
             pltpu.VMEM((blocks, batch, LANES), BF16),
             pltpu.VMEM((n_tp, 8, LANES), BF16),
             pltpu.VMEM((n_tp, 8, LANES), BF16),
             pltpu.SemaphoreType.DMA((3 + 3 * layers,)),
-            pltpu.SemaphoreType.DMA((2 * layers + 4,)),
-            pltpu.SemaphoreType.DMA((2 * layers + 4,)),
+            pltpu.SemaphoreType.DMA((2 * layers + 5,)),
+            pltpu.SemaphoreType.DMA((2 * layers + 5,)),
             pltpu.SemaphoreType.REGULAR((2,)),
         ],
         compiler_params=pltpu.CompilerParams(collective_id=0, has_side_effects=True),

time: 102 us -> 100 us (0.980)
  Pallas kernels: 101 us -> 99.1 us
    pallas_call x1, Pallas kernels: 100 us -> 98.1 us  [body(): pl.pallas_call(functools.partial(kernel, n_tp, n_dp), out_shape=kept, in_...]
where the time goes in v5:
time: 100 us; the launch traced here: 99.8 us
  Pallas kernels  99.1 us (99%)
    pallas_call x1, Pallas kernels, body(): pl.pallas_call(functools.partial(kernel, n_tp, n_dp), out_shape=kept, in_...  98.1 us

profile of v5, /device:TPU:40, one launch (start us, length us, event | category | flops | bytes accessed | tf_op | source)
XLA Modules:
  0.0 99.8 jit_solution(6160286588850043036)
XLA Ops:
  0.6 98.1 %shard_map.184 = (bf16[2,512]{1,0:T(2,128)(2,1)S(1)}, f32[2,8,2,64,128]{4,3,2,1,0:T(8,128)S(1)}, bf16[2,8,3,4,128]{4,3,2,1,0:T(4,128)(2,1)S(1)}) custom-call(bf16[64,512]{1,0:T(8,128)(2,1)} %h_in.1, s32[8]{0:T(128)} %counts_in.1, f32[2,512]{1,0:T(2,128)} %in_gain_in.1, bf16[2,512,128]{2,1,0:T(8,128)(2,1)} %w_value.1, bf16[2,512,128]{2,1,0:T(8,128)(2,1)} %w_inkey.1, ...), custom_call_target="tpu_custom_call" | custom-call | tf_op jit(solution)/shard_map/pallas_call | solution.py:519
  98.8 1.0 %shard_map.185 = (bf16[2,512]{1,0:T(2,128)(2,1)}, f32[2,8,2,64,128]{4,3,2,1,0:T(8,128)}, bf16[2,8,3,4,128]{4,3,2,1,0:T(4,128)(2,1)}) custom-call(bf16[2,512]{1,0:T(2,128)(2,1)S(1)} %get-tuple-element.9.hidden_v, f32[2,8,2,64,128]{4,3,2,1,0:T(8,128)S(1)} %get-tuple-element.10.states_v, bf16[2,8,3,4,128]{4,3,2,1,0:T(4,128)(2,1)S(1)} %get-tuple-element.11.windows_v), custom_call_target="tpu_custom_call" | custom-call | tf_op jit(solution)/shard_map/pallas_call | solution.py:557

commit v6 on v5

--- a/solution.py
+++ b/solution.py
@@ -353,10 +353,10 @@
         with jax.named_scope("pair_send"):
             far_recv[me_pair] = (pair_v[0].astype(F32) + pair_v[1].astype(F32)).astype(BF16)
             pl.semaphore_wait(know_sem.at[1], 2)
-            for step in range(far // 2, 0, -1):
-                for shift in sorted({step, far - step}):
-                    to = tp_at(shift * 2 * blocks)
-                    remote(far_recv.at[me_pair], far_recv.at[me_pair], far_sum, to)
+            for step in range(far - 1, 0, -1):
+                away = step * blocks * (2 * odd - 1)
+                to = {"tp": lax.rem(me_tp + n_tp + away, n_tp)}
+                remote(far_recv.at[me_pair], far_recv.at[me_pair], far_sum, to)
         with jax.named_scope("far_wait"):
             total_wait(far_recv, far - 1, recv_sem.at[far_sum])
         with jax.named_scope("near_all"):

time: 100 us -> 98.8 us (0.988)
  Pallas kernels: 99.1 us -> 98 us
    pallas_call x1, Pallas kernels: 98.1 us -> 97 us  [body(): pl.pallas_call(functools.partial(kernel, n_tp, n_dp), out_shape=kept, in_...]
where the time goes in v6:
time: 98.8 us; the launch traced here: 98.7 us
  Pallas kernels  98 us (99%)
    pallas_call x1, Pallas kernels, body(): pl.pallas_call(functools.partial(kernel, n_tp, n_dp), out_shape=kept, in_...  97 us

profile of v6, /device:TPU:40, one launch (start us, length us, event | category | flops | bytes accessed | tf_op | source)
XLA Modules:
  0.0 98.7 jit_solution(14433998291965030865)
XLA Ops:
  0.6 97.0 %shard_map.184 = (bf16[2,512]{1,0:T(2,128)(2,1)S(1)}, f32[2,8,2,64,128]{4,3,2,1,0:T(8,128)S(1)}, bf16[2,8,3,4,128]{4,3,2,1,0:T(4,128)(2,1)S(1)}) custom-call(bf16[64,512]{1,0:T(8,128)(2,1)} %h_in.1, s32[8]{0:T(128)} %counts_in.1, f32[2,512]{1,0:T(2,128)} %in_gain_in.1, bf16[2,512,128]{2,1,0:T(8,128)(2,1)} %w_value.1, bf16[2,512,128]{2,1,0:T(8,128)(2,1)} %w_inkey.1, ...), custom_call_target="tpu_custom_call" | custom-call | tf_op jit(solution)/shard_map/pallas_call | solution.py:519
  97.6 1.0 %shard_map.185 = (bf16[2,512]{1,0:T(2,128)(2,1)}, f32[2,8,2,64,128]{4,3,2,1,0:T(8,128)}, bf16[2,8,3,4,128]{4,3,2,1,0:T(4,128)(2,1)}) custom-call(bf16[2,512]{1,0:T(2,128)(2,1)S(1)} %get-tuple-element.9.hidden_v, f32[2,8,2,64,128]{4,3,2,1,0:T(8,128)S(1)} %get-tuple-element.10.states_v, bf16[2,8,3,4,128]{4,3,2,1,0:T(4,128)(2,1)S(1)} %get-tuple-element.11.windows_v), custom_call_target="tpu_custom_call" | custom-call | tf_op jit(solution)/shard_map/pallas_call | solution.py:557

commit v7 on v6

--- a/solution.py
+++ b/solution.py
@@ -14,6 +14,7 @@
 BF16 = jnp.bfloat16
 LANES = 128
 STAT = 3
+SPACING = 2000
 
 
 def total_wait(buffer, count, sem):
@@ -99,8 +100,15 @@
     def dp_at(shift):
         return {"dp": lax.rem(me_dp + shift, n_dp)}
 
-    def near_at(shift):
-        return {"tp": me_block * blocks + lax.rem(me_quarter + shift, blocks)}
+    near = [
+        blocks - 1 - me_quarter,
+        me_quarter + 2 - 4 * (me_quarter // 2),
+        me_quarter + 1 - 2 * lax.rem(me_quarter, 2),
+    ]
+    assert blocks == len(near) + 1
+
+    def near_at(quarter):
+        return {"tp": me_block * blocks + quarter}
 
     def remote(source, target, sem, to):
         pltpu.make_async_remote_copy(
@@ -308,10 +316,10 @@
         if l + 1 < layers:
             here = wide_recv.at[me_quarter * n_dp + me_dp]
             for shift in dp_shifts:
-                for near in range(1, blocks):
-                    remote(here, here, mix_at(l), near_at(near) | dp_at(shift))
-            for near in range(1, blocks):
-                remote(here, here, mix_at(l), near_at(near))
+                for quarter in near:
+                    remote(here, here, mix_at(l), near_at(quarter) | dp_at(shift))
+            for quarter in near:
+                remote(here, here, mix_at(l), near_at(quarter))
         else:
             here = mix_recv.at[me_dp]
         for shift in dp_shifts:
@@ -324,10 +332,9 @@
             total_wait(mix_recv, n_dp - 1, sem)
 
     def send_weights():
-        for near in range(1, blocks):
-            quarter = lax.rem(me_quarter + near, blocks)
+        for quarter in near:
             columns = pl.ds(pl.multiple_of(quarter * LANES, LANES), LANES)
-            remote(wo_v.at[0, :, columns], wo_near.at[me_quarter], weights_near, near_at(near))
+            remote(wo_v.at[0, :, columns], wo_near.at[me_quarter], weights_near, near_at(quarter))
         columns = pl.ds(pl.multiple_of(me_quarter * LANES, LANES), LANES)
         wo_near[me_quarter] = wo_v[0, :, columns]
 
@@ -354,6 +361,8 @@
             far_recv[me_pair] = (pair_v[0].astype(F32) + pair_v[1].astype(F32)).astype(BF16)
             pl.semaphore_wait(know_sem.at[1], 2)
             for step in range(far - 1, 0, -1):
+                if step < far - 1:
+                    pl.delay(SPACING)
                 away = step * blocks * (2 * odd - 1)
                 to = {"tp": lax.rem(me_tp + n_tp + away, n_tp)}
                 remote(far_recv.at[me_pair], far_recv.at[me_pair], far_sum, to)
@@ -362,8 +371,8 @@
         with jax.named_scope("near_all"):
             mine = (h + jnp.sum(far_recv[...].astype(F32), axis=0)).astype(BF16)
             own_recv[me_quarter] = mine
-            for shift in range(1, blocks):
-                remote(own_recv.at[me_quarter], own_recv.at[me_quarter], near_all, near_at(shift))
+            for quarter in near:
+                remote(own_recv.at[me_quarter], own_recv.at[me_quarter], near_all, near_at(quarter))
         with jax.named_scope("near_all_wait"):
             total_wait(own_recv, blocks - 1, recv_sem.at[near_all])
         return jnp.concatenate([own_recv[j].astype(F32) for j in range(blocks)], axis=1)

time: 98.8 us -> 96.2 us (0.974)
  Pallas kernels: 98 us -> 95.4 us
    pallas_call x1, Pallas kernels: 97 us -> 94.4 us  [body(): pl.pallas_call(functools.partial(kernel, n_tp, n_dp), out_shape=kept, in_...]
where the time goes in v7:
time: 96.2 us; the launch traced here: 96 us
  Pallas kernels  95.4 us (99%)
    pallas_call x1, Pallas kernels, body(): pl.pallas_call(functools.partial(kernel, n_tp, n_dp), out_shape=kept, in_...  94.4 us

profile of v7, /device:TPU:40, one launch (start us, length us, event | category | flops | bytes accessed | tf_op | source)
XLA Modules:
  0.0 96.0 jit_solution(4260420145905812442)
XLA Ops:
  0.6 94.4 %shard_map.184 = (bf16[2,512]{1,0:T(2,128)(2,1)S(1)}, f32[2,8,2,64,128]{4,3,2,1,0:T(8,128)S(1)}, bf16[2,8,3,4,128]{4,3,2,1,0:T(4,128)(2,1)S(1)}) custom-call(bf16[64,512]{1,0:T(8,128)(2,1)} %h_in.1, s32[8]{0:T(128)} %counts_in.1, f32[2,512]{1,0:T(2,128)} %in_gain_in.1, bf16[2,512,128]{2,1,0:T(8,128)(2,1)} %w_value.1, bf16[2,512,128]{2,1,0:T(8,128)(2,1)} %w_inkey.1, ...), custom_call_target="tpu_custom_call" | custom-call | tf_op jit(solution)/shard_map/pallas_call | solution.py:528
  95.0 1.0 %shard_map.185 = (bf16[2,512]{1,0:T(2,128)(2,1)}, f32[2,8,2,64,128]{4,3,2,1,0:T(8,128)}, bf16[2,8,3,4,128]{4,3,2,1,0:T(4,128)(2,1)}) custom-call(bf16[2,512]{1,0:T(2,128)(2,1)S(1)} %get-tuple-element.9.hidden_v, f32[2,8,2,64,128]{4,3,2,1,0:T(8,128)S(1)} %get-tuple-element.10.states_v, bf16[2,8,3,4,128]{4,3,2,1,0:T(4,128)(2,1)S(1)} %get-tuple-element.11.windows_v), custom_call_target="tpu_custom_call" | custom-call | tf_op jit(solution)/shard_map/pallas_call | solution.py:566

commit v8 on v7

--- a/solution.py
+++ b/solution.py
@@ -266,19 +266,23 @@
             decay = jnp.exp(-rate * fixed_v[l, 1] + fixed_v[l, 0])
             gain = rate * value
             high, low = halves(gain)
-            none = jnp.zeros((LANES - 3 * rows, LANES), BF16)
-            parts = jnp.concatenate([high, high, low, none], axis=0)
+            none = jnp.zeros((rows, LANES), F32)
+            parts = jnp.concatenate([high, high, low, none.astype(BF16)], axis=0)
             columns = lax.dot_general(
                 unit, parts, (((1,), (1,)), ((), ())), preferred_element_type=F32
-            )
-            lane_sq = lax.broadcasted_iota(jnp.int32, (LANES, LANES), 1)
-            left = jnp.concatenate(
-                [jnp.where(lane_sq % rows == b, columns, 0.0).astype(BF16) for b in range(rows)],
-                axis=0,
-            )
-            high, low = halves(inkey)
-            right = jnp.concatenate([high, low, high, none], axis=0)
-            outer = jnp.dot(left, right, preferred_element_type=F32)
+            ).astype(BF16)
+            high, low = (half.astype(F32) for half in halves(inkey))
+            right = jnp.concatenate(
+                [
+                    jnp.concatenate(
+                        [jnp.where(sub == b, half, 0.0) for half in (high, low, high)] + [none],
+                        axis=0,
+                    )
+                    for b in range(rows)
+                ],
+                axis=1,
+            ).astype(BF16)
+            outer = jnp.dot(columns, right, preferred_element_type=F32)
             reader = readkey.astype(BF16)
             fades = [
                 jnp.broadcast_to(decay[:, k * head_dim : k * head_dim + 1], (rows, LANES))
@@ -288,8 +292,10 @@
             for b in range(rows):
                 news = []
                 for k in range(heads):
-                    at = (b * heads + k) * head_dim
-                    new = fades[k][b : b + 1] * state_v[l, b, k] + outer[at : at + head_dim]
+                    added = outer[
+                        k * head_dim : (k + 1) * head_dim, b * LANES : (b + 1) * LANES
+                    ]
+                    new = fades[k][b : b + 1] * state_v[l, b, k] + added
                     state_out[l, b, k] = new
                     news.append(new.astype(BF16))
                 read = lax.dot_general(
@@ -371,7 +377,9 @@
         with jax.named_scope("near_all"):
             mine = (h + jnp.sum(far_recv[...].astype(F32), axis=0)).astype(BF16)
             own_recv[me_quarter] = mine
-            for quarter in near:
+            for n, quarter in enumerate(near):
+                if n:
+                    pl.delay(SPACING // 3)
                 remote(own_recv.at[me_quarter], own_recv.at[me_quarter], near_all, near_at(quarter))
         with jax.named_scope("near_all_wait"):
             total_wait(own_recv, blocks - 1, recv_sem.at[near_all])

time: 96.2 us -> 96.2 us (level)
  no operation moved by 1% of the time
where the time goes in v8:
time: 96.2 us; the launch traced here: 96 us
  Pallas kernels  95.4 us (99%)
    pallas_call x1, Pallas kernels, body(): pl.pallas_call(functools.partial(kernel, n_tp, n_dp), out_shape=kept, in_...  94.3 us

profile of v8, /device:TPU:40, one launch (start us, length us, event | category | flops | bytes accessed | tf_op | source)
XLA Modules:
  0.0 96.0 jit_solution(14422926343514142970)
XLA Ops:
  0.6 94.3 %shard_map.184 = (bf16[2,512]{1,0:T(2,128)(2,1)S(1)}, f32[2,8,2,64,128]{4,3,2,1,0:T(8,128)S(1)}, bf16[2,8,3,4,128]{4,3,2,1,0:T(4,128)(2,1)S(1)}) custom-call(bf16[64,512]{1,0:T(8,128)(2,1)} %h_in.1, s32[8]{0:T(128)} %counts_in.1, f32[2,512]{1,0:T(2,128)} %in_gain_in.1, bf16[2,512,128]{2,1,0:T(8,128)(2,1)} %w_value.1, bf16[2,512,128]{2,1,0:T(8,128)(2,1)} %w_inkey.1, ...), custom_call_target="tpu_custom_call" | custom-call | tf_op jit(solution)/shard_map/pallas_call | solution.py:536
  95.0 1.0 %shard_map.185 = (bf16[2,512]{1,0:T(2,128)(2,1)}, f32[2,8,2,64,128]{4,3,2,1,0:T(8,128)}, bf16[2,8,3,4,128]{4,3,2,1,0:T(4,128)(2,1)}) custom-call(bf16[2,512]{1,0:T(2,128)(2,1)S(1)} %get-tuple-element.9.hidden_v, f32[2,8,2,64,128]{4,3,2,1,0:T(8,128)S(1)} %get-tuple-element.10.states_v, bf16[2,8,3,4,128]{4,3,2,1,0:T(4,128)(2,1)S(1)} %get-tuple-element.11.windows_v), custom_call_target="tpu_custom_call" | custom-call | tf_op jit(solution)/shard_map/pallas_call | solution.py:574
